TPU v7x, 512 devices: a whole 4x4x16 slice. The times are simulated.
512 devices in a mesh: ep: 32 (over z, core), tp: 16 (over y, x).
Axes of the slice: x: 4, y: 4, z: 16, core: 2. Of those that a mesh axis runs over, the one named last changes fastest.
Arguments:
- query_maps: bfloat16 [8192, 4096], P('ep', 'tp'), may hold values from -40 to 40
- key_maps: bfloat16 [8192, 4096], P('ep', 'tp'), may hold values from -40 to 40
- value_rows: bfloat16 [8192, 4096], P('ep', 'tp'), may hold values from -6 to 6
- head_lambda: float32 [16], P('tp'), may hold values from 0.3 to 0.8
- head_gain: float32 [256], replicated, may hold values from 0.1 to 1.9
- out_weight: bfloat16 [4096, 2048], P('tp'), may hold values from -0.125 to 0.125
- expert_rows: bfloat16 [4096, 2048], P('ep'), may hold values from -6 to 6
- expert_gain: float32 [2048], replicated, may hold values from 0.1 to 1.9
- routes: int32 [4096, 2], P('ep'), may hold values from 0 to 31, all different within a row; in each aligned block of 128 rows (0 to 127, 128 to 255, ...) at most 12 rows name the same one
- route_weights: float32 [4096, 2], P('ep'), may hold values from 0.2 to 1
- gate_weight: bfloat16 [32, 2048, 4096], P('ep', None, 'tp'), may hold values from -0.125 to 0.125
- up_weight: bfloat16 [32, 2048, 4096], P('ep', None, 'tp'), may hold values from -0.125 to 0.125
- down_weight: bfloat16 [32, 4096, 2048], P('ep', 'tp'), may hold values from -0.125 to 0.125
Outputs:
- mixed: bfloat16 [8192, 2048], P('ep', 'tp')
- expert_out: bfloat16 [4096, 2048], P('ep', 'tp')
Inputs may be any that keep to these rules, and one draw needn't show every extreme that they name: `routes`: within the rows of one device (aligned blocks of 128 rows) no expert is named more than 12 times, and the 2 experts of a row differ.
All inputs are finite; a program needn't handle non-finite values.
Results may differ from a plain program's by a relative error of at most 0.018.
Values may be sent and summed in bfloat16 or wider, within the bound.
A program may use at most 128 MiB of HBM per device.

v0:
```python
import jax
import jax.numpy as jnp
from jax import lax
from jax.sharding import PartitionSpec as P

norm_eps = 1e-06
rope_base = 10000.0


def side_by_side(arrays, axis, dim, along):
    both = jnp.concatenate(arrays, axis=along)
    whole, at, finished = (lax.all_gather(both, axis, axis=dim, tiled=True), 0, [])
    for a in arrays:
        finished.append(lax.slice_in_dim(whole, at, at + a.shape[along], axis=along))
        at += a.shape[along]
    return tuple(finished)


def in_blocks(shard, dim, peers):
    lengths = shard.shape
    parts = shard.reshape(*lengths[:dim], peers, lengths[dim] // peers, *lengths[dim + 1 :])
    return jnp.moveaxis(parts, dim, 0)


def sum_at_owner(shard, axis, dim):
    parts = in_blocks(shard, dim, lax.axis_size(axis))
    arrived = lax.all_to_all(parts, axis, split_axis=0, concat_axis=0, tiled=True)
    return arrived.astype(jnp.float32).sum(axis=0)


def in_order(parts, dim):
    parts = jnp.moveaxis(parts, 0, dim)
    lengths = parts.shape
    return parts.reshape(*lengths[:dim], lengths[dim] * lengths[dim + 1], *lengths[dim + 2 :])


def copy_for_each(shard, axis):
    peers = lax.axis_size(axis)
    return lax.all_to_all(
        jnp.broadcast_to(shard[None], (peers, *shard.shape)), axis, 0, 0, tiled=True
    )


def collect(shard, axis, dim):
    return in_order(copy_for_each(shard, axis), dim)


def rope_turn(inputs, positions):
    half_dim = inputs.shape[-1] // 2
    inverse = rope_base ** (-2.0 * jnp.arange(half_dim, dtype=jnp.float32) / inputs.shape[-1])
    angles = positions.astype(jnp.float32)[:, None] * inverse[None, :]
    cos_table = jnp.cos(angles)[:, None, None, :]
    sin_table = jnp.sin(angles)[:, None, None, :]
    first_half = inputs[..., :half_dim]
    second_half = inputs[..., half_dim:]
    return jnp.concatenate(
        [
            first_half * cos_table - second_half * sin_table,
            second_half * cos_table + first_half * sin_table,
        ],
        axis=-1,
    )


def mixer_half(query_maps, key_maps, value_rows, head_lambda, head_gain, out_weight):
    row_count = query_maps.shape[0]
    head_count = head_lambda.shape[0]
    head_dim = query_maps.shape[1] // (2 * head_count)
    value_dim = value_rows.shape[1] // head_count
    model_width = out_weight.shape[1]
    score_scale = head_dim ** (-0.5)
    offset = lax.axis_index("ep") * row_count
    positions = offset + jnp.arange(row_count, dtype=jnp.int32)
    last_row = offset + row_count - 1
    rotated_q = rope_turn(
        query_maps.astype(jnp.float32).reshape(row_count, head_count, 2, head_dim), positions
    ).astype(jnp.bfloat16)
    rotated_k = rope_turn(
        key_maps.astype(jnp.float32).reshape(row_count, head_count, 2, head_dim), positions
    ).astype(jnp.bfloat16)
    rotated_k = rotated_k.reshape(row_count, head_count * 2 * head_dim)
    initial = (
        jnp.full((head_count, 2, row_count), -1e30, jnp.float32),
        jnp.zeros((head_count, 2, row_count), jnp.float32),
        jnp.zeros((head_count, 2, row_count, value_dim), jnp.float32),
    )
    piece_k, piece_v = side_by_side((rotated_k, value_rows), "ep", 0, 1)
    piece_len = piece_k.shape[0]
    block_size = 1024

    def attend(state):

        def fold_step(inner, block_index):
            block_start = block_index * block_size
            block_k = lax.dynamic_slice_in_dim(piece_k, block_start, block_size, 0).reshape(
                block_size, head_count, 2, head_dim
            )
            block_v = lax.dynamic_slice_in_dim(piece_v, block_start, block_size, 0).reshape(
                block_size, head_count, value_dim
            )
            scores = (
                jnp.einsum(
                    "qhmd,khmd->hmqk", rotated_q, block_k, preferred_element_type=jnp.float32
                )
                * score_scale
            )
            key_pos = block_start + jnp.arange(block_size, dtype=jnp.int32)
            causal = key_pos[None, :] <= positions[:, None]
            masked = jnp.where(causal, scores, -1e30)
            run_max, run_sum, run_acc = inner
            new_max = jnp.maximum(run_max, jnp.max(masked, axis=-1))
            expd = jnp.where(causal, jnp.exp(masked - new_max[..., None]), 0.0)
            rescale = jnp.exp(run_max - new_max)
            new_sum = run_sum * rescale + jnp.sum(expd, axis=-1)
            new_acc = run_acc * rescale[..., None] + jnp.einsum(
                "hmqk,khe->hmqe",
                expd.astype(jnp.bfloat16),
                block_v,
                preferred_element_type=jnp.float32,
            )
            return ((new_max, new_sum, new_acc), None)

        result, _ = lax.scan(fold_step, state, jnp.arange(piece_len // block_size, dtype=jnp.int32))
        return result

    def skip_piece(state):
        return state

    run_max, run_sum, run_acc = lax.cond(jnp.int32(0) <= last_row, attend, skip_piece, initial)
    first_map = run_acc[:, 0] / run_sum[:, 0][..., None]
    second_map = run_acc[:, 1] / run_sum[:, 1][..., None]
    difference = first_map - head_lambda[:, None, None] * second_map
    head_out = (
        difference
        * lax.rsqrt(jnp.mean(difference * difference, axis=-1, keepdims=True) + norm_eps)
        * head_gain
    ).astype(jnp.bfloat16)
    partial_value = jnp.einsum(
        "hqe,hed->qd",
        head_out,
        out_weight.reshape(head_count, value_dim, model_width),
        preferred_element_type=jnp.float32,
    )
    return sum_at_owner(partial_value.astype(jnp.bfloat16), "tp", 1).astype(jnp.bfloat16)


def expert_half(
    expert_rows, expert_gain, routes, route_weights, gate_weight, up_weight, down_weight
):
    ep_count = lax.axis_size("ep")
    tp_count = lax.axis_size("tp")
    row_count, model_width = expert_rows.shape
    pick_count = routes.shape[1]
    capacity = 3 * row_count * pick_count // (2 * ep_count)
    column_count = model_width // tp_count
    inputs = expert_rows.astype(jnp.float32)
    normed = (
        inputs
        * lax.rsqrt(jnp.mean(inputs * inputs, axis=-1, keepdims=True) + norm_eps)
        * expert_gain
    ).astype(jnp.bfloat16)
    expert_ids = routes.reshape(-1)
    one_hot = (expert_ids[:, None] == jnp.arange(ep_count, dtype=jnp.int32)[None, :]).astype(
        jnp.int32
    )
    slot_index = jnp.sum((jnp.cumsum(one_hot, axis=0) - one_hot) * one_hot, axis=1)
    source_row = jnp.arange(row_count * pick_count, dtype=jnp.int32) // pick_count
    sent = lax.dynamic_slice_in_dim(normed, lax.axis_index("tp") * column_count, column_count, 1)
    empty = jnp.zeros((ep_count, capacity, sent.shape[1]), jnp.bfloat16)
    arrived = collect(
        lax.all_to_all(
            empty.at[expert_ids, slot_index].set(sent[source_row]),
            "ep",
            split_axis=0,
            concat_axis=0,
            tiled=True,
        ),
        "tp",
        2,
    )
    slot_count = arrived.shape[1]
    flat_rows = arrived.reshape(ep_count * slot_count, model_width)
    gate_values = jnp.dot(flat_rows, gate_weight[0], preferred_element_type=jnp.float32)
    up_values = jnp.dot(flat_rows, up_weight[0], preferred_element_type=jnp.float32)
    hidden = (jax.nn.silu(gate_values) * up_values).astype(jnp.bfloat16)
    partial_value = jnp.dot(hidden, down_weight[0], preferred_element_type=jnp.float32).reshape(
        ep_count, slot_count, model_width
    )
    summed = sum_at_owner(partial_value.astype(jnp.bfloat16), "tp", 2).astype(jnp.bfloat16)
    returned = lax.all_to_all(summed, "ep", split_axis=0, concat_axis=0, tiled=True)
    picked = returned[expert_ids, slot_index].reshape(row_count, pick_count, column_count)
    combined = jnp.sum(route_weights[..., None] * picked.astype(jnp.float32), axis=1)
    return combined.astype(jnp.bfloat16)


def on_device(
    query_maps,
    key_maps,
    value_rows,
    head_lambda,
    head_gain,
    out_weight,
    expert_rows,
    expert_gain,
    routes,
    route_weights,
    gate_weight,
    up_weight,
    down_weight,
):
    mixed = mixer_half(query_maps, key_maps, value_rows, head_lambda, head_gain, out_weight)
    expert_out = expert_half(
        expert_rows, expert_gain, routes, route_weights, gate_weight, up_weight, down_weight
    )
    return (mixed, expert_out)


def solution(mesh):
    placed = (
        P("ep", "tp"),
        P("ep", "tp"),
        P("ep", "tp"),
        P("tp"),
        P(),
        P("tp", None),
        P("ep", None),
        P(),
        P("ep", None),
        P("ep", None),
        P("ep", None, "tp"),
        P("ep", None, "tp"),
        P("ep", "tp", None),
    )
    return jax.shard_map(
        on_device,
        mesh=mesh,
        in_specs=placed,
        out_specs=(P("ep", "tp"), P("ep", "tp")),
        check_vma=False,
    )
```

profile of v0, /device:TPU:32, one launch (start us, length us, event | category | flops | bytes accessed | tf_op | source)
XLA Modules:
  0.0 243.4 jit_solution(10236540389704936372)
XLA Ops:
  7.3 1.1 copy.56
  8.4 1.0 copy.58
  9.5 1.0 copy.57
  10.9 0.7 pad_maximum_fusion
  12.3 0.6 reduce-window.6
  13.1 0.8 dynamic-slice
  14.2 0.9 gather_fusion
  15.2 12.3 %scatter_fusion = bf16[32,12,128]{2,0,1:T(8,128)(2,1)S(1)} fusion(bf16[32,12,128]{2,0,1:T(8,128)(2,1)S(1)} %broadcast_in_dim.38, s32[256]{0:T(256)S(1)} %bitcast.171, bf16[256,128]{1,0:T(8,128)(2,1)S(1)} %gather_fusion), kind=kCustom, calls=%fused_computation.2 | custom fusion | bytes 198656 | tf_op jit(solution)/shard_map/scatter | solution.py:172
  27.5 31.1 %all_to_all.25 = bf16[32,12,128]{2,1,0:T(8,128)(2,1)S(1)} all-to-all(bf16[32,12,128]{2,1,0:T(8,128)(2,1)S(1)} %copy.67), channel_id=1, replica_groups=mesh['ep'=32,'tp'=16] {'ep'}, dimensions={0} | all-to-all | bytes 196608 | tf_op jit(solution)/shard_map/all_to_all | solution.py:171
  59.0 29.5 %all_to_all.26 = bf16[16,32,12,128]{3,1,2,0:T(8,128)(2,1)S(1)} all-to-all(bf16[16,32,12,128]{3,1,2,0:T(8,128)(2,1)S(1)} %broadcast_in_dim.39), channel_id=1, replica_groups=mesh['ep'=32,'tp'=16] {'tp'}, dimensions={0} | all-to-all | bytes 3145728 | tf_op jit(solution)/shard_map/all_to_all | solution.py:39
  88.4 1.0 copy.69
  89.6 0.6 fusion.20
  90.7 0.6 fusion.29
  91.4 0.6 fusion.22
  92.0 1.6 copy.99
  93.6 3.7 %all-to-all-start.3 = ((bf16[16,32,12,128]{3,1,2,0:T(8,128)(2,1)}), bf16[16,32,12,128]{3,1,2,0:T(8,128)(2,1)S(1)}, u32[]{:S(2)}, u32[]{:S(2)}) async-start(bf16[16,32,12,128]{3,1,2,0:T(8,128)(2,1)} %bitcast.173), calls=%async_computation.3 | async-start | bytes 3145728 | tf_op jit(solution)/shard_map/all_to_all | solution.py:27
  98.0 21.0 %all-to-all-done.3 = bf16[16,32,12,128]{3,1,2,0:T(8,128)(2,1)S(1)} async-done(((bf16[16,32,12,128]{3,1,2,0:T(8,128)(2,1)}), bf16[16,32,12,128]{3,1,2,0:T(8,128)(2,1)S(1)}, u32[]{:S(2)}, u32[]{:S(2)}) %all-to-all-start.3) | async-done | bytes 1572896 | tf_op jit(solution)/shard_map/all_to_all | solution.py:27
  119.2 0.7 copy.72
  119.9 7.5 %all-to-all-start.4 = ((bf16[32,12,128]{2,1,0:T(8,128)(2,1)}), bf16[32,12,128]{2,1,0:T(8,128)(2,1)}, u32[]{:S(2)}, u32[]{:S(2)}) async-start(bf16[32,12,128]{2,1,0:T(8,128)(2,1)} %copy.72), calls=%async_computation.4 | async-start | bytes 262144 | tf_op jit(solution)/shard_map/all_to_all | solution.py:190
  127.5 81.2 %conditional.1 = (f32[256]{0:T(256)S(1)}, f32[256]{0:T(256)S(1)}, f32[1,1,256,256]{3,2,1,0:T(8,128)}, f32[1,1,256,256]{3,2,1,0:T(8,128)}) conditional(s32[]{:T(128)} %convert_element_type.75, () %tuple.26, (bf16[8192,512]{0,1:T(8,128)(2,1)}, s32[]{:T(128)}, s32[256]{0:T(256)S(1)}, bf16[256,1,2,128]{0,3,2,1:T(8,128)(2,1)S(1)}) %tuple.27), branch_computations={%region_0.0_spmd.clone, %region_1.6_spmd.clone} | conditional | flops 410128640 | bytes 79093208 | solution.py:129
  127.5 11.9 %copy.76 = bf16[8192,512]{1,0:T(8,128)(2,1)} copy(bf16[8192,512]{0,1:T(8,128)(2,1)} %get-tuple-element.138) | data formatting | bytes 16777216 | tf_op jit(solution)/shard_map
  139.4 4.7 %slice.72 = bf16[8192,256]{1,0:T(8,128)(2,1)} slice(bf16[8192,512]{1,0:T(8,128)(2,1)} %copy.76), slice={[0:8192], [256:512]} | slice | bytes 8388608 | tf_op jit(solution)/shard_map/slice | solution.py:14
  144.2 1.4 copy-done.1
  145.6 2.3 slice.64
  148.6 58.3 %while.19 = (s32[]{:T(128)}, f32[1,2,256]{2,1,0:T(2,128)S(1)}, f32[1,2,256]{2,1,0:T(2,128)S(1)}, f32[1,2,256,256]{3,2,1,0:T(8,128)}, s32[8]{0:T(128)}, /*index=5...) while((s32[]{:T(128)}, f32[1,2,256]{2,1,0:T(2,128)S(1)}, ...), condition=%wide.region_5.5_spmd.clone, body=%wide.region_2.4_spmd.clone.sunk | while | flops 410128384 | bytes 10667271 | solution.py:123
  148.6 1.2 dynamic_slice.33
  150.4 1.1 constant_dynamic-slice_fusion.2
  152.3 2.7 %fusion.77 = f32[1,2,256,256]{3,2,1,0:T(8,128)} fusion(f32[2,1024,256]{2,1,0:T(8,128)S(1)} %get-tuple-element.243, f32[2,256]{1,0:T(2,128)S(1)} %bitcast.177, pred[256,1024]{0,1:T(8,128)(4,1)S(1)} %broadcast_compare_fusion.2, f32[1,2,256,256]{3,2,1,0:T(8,128)} %get-tuple-element.261, bf16[8192,256]{1,0:T(8,128)(2,1)} %get-tuple-element.279, ...), kind=kOutput, calls=%fused_computation.9.clone.1 | convolution fusion | flops 271450112 | bytes 3936261 | tf_op jit(solution)/shard_map/cond/branch_1_fun/while/body/eval_jaxpr/hmqk,khe->hmqe/dot_general | solution.py:115
  155.0 0.6 fusion.76
  155.7 1.2 dynamic_slice.33
  157.6 1.1 constant_dynamic-slice_fusion.2
  159.5 2.9 %fusion.77 = f32[1,2,256,256]{3,2,1,0:T(8,128)} fusion(f32[2,1024,256]{2,1,0:T(8,128)S(1)} %get-tuple-element.243, f32[2,256]{1,0:T(2,128)S(1)} %bitcast.177, pred[256,1024]{0,1:T(8,128)(4,1)S(1)} %broadcast_compare_fusion.2, f32[1,2,256,256]{3,2,1,0:T(8,128)} %get-tuple-element.261, bf16[8192,256]{1,0:T(8,128)(2,1)} %get-tuple-element.279, ...), kind=kOutput, calls=%fused_computation.9.clone.1 | convolution fusion | flops 271450112 | bytes 3936261 | tf_op jit(solution)/shard_map/cond/branch_1_fun/while/body/eval_jaxpr/hmqk,khe->hmqe/dot_general | solution.py:115
  162.3 0.6 fusion.76
  163.0 1.2 dynamic_slice.33
  164.9 1.1 constant_dynamic-slice_fusion.2
  166.8 2.9 %fusion.77 = f32[1,2,256,256]{3,2,1,0:T(8,128)} fusion(f32[2,1024,256]{2,1,0:T(8,128)S(1)} %get-tuple-element.243, f32[2,256]{1,0:T(2,128)S(1)} %bitcast.177, pred[256,1024]{0,1:T(8,128)(4,1)S(1)} %broadcast_compare_fusion.2, f32[1,2,256,256]{3,2,1,0:T(8,128)} %get-tuple-element.261, bf16[8192,256]{1,0:T(8,128)(2,1)} %get-tuple-element.279, ...), kind=kOutput, calls=%fused_computation.9.clone.1 | convolution fusion | flops 271450112 | bytes 3936261 | tf_op jit(solution)/shard_map/cond/branch_1_fun/while/body/eval_jaxpr/hmqk,khe->hmqe/dot_general | solution.py:115
  170.3 1.2 dynamic_slice.33
  172.2 1.1 constant_dynamic-slice_fusion.2
  174.1 2.9 %fusion.77 = f32[1,2,256,256]{3,2,1,0:T(8,128)} fusion(f32[2,1024,256]{2,1,0:T(8,128)S(1)} %get-tuple-element.243, f32[2,256]{1,0:T(2,128)S(1)} %bitcast.177, pred[256,1024]{0,1:T(8,128)(4,1)S(1)} %broadcast_compare_fusion.2, f32[1,2,256,256]{3,2,1,0:T(8,128)} %get-tuple-element.261, bf16[8192,256]{1,0:T(8,128)(2,1)} %get-tuple-element.279, ...), kind=kOutput, calls=%fused_computation.9.clone.1 | convolution fusion | flops 271450112 | bytes 3936261 | tf_op jit(solution)/shard_map/cond/branch_1_fun/while/body/eval_jaxpr/hmqk,khe->hmqe/dot_general | solution.py:115
  176.9 0.6 fusion.76
  177.6 1.2 dynamic_slice.33
  179.5 1.1 constant_dynamic-slice_fusion.2
  181.4 2.9 %fusion.77 = f32[1,2,256,256]{3,2,1,0:T(8,128)} fusion(f32[2,1024,256]{2,1,0:T(8,128)S(1)} %get-tuple-element.243, f32[2,256]{1,0:T(2,128)S(1)} %bitcast.177, pred[256,1024]{0,1:T(8,128)(4,1)S(1)} %broadcast_compare_fusion.2, f32[1,2,256,256]{3,2,1,0:T(8,128)} %get-tuple-element.261, bf16[8192,256]{1,0:T(8,128)(2,1)} %get-tuple-element.279, ...), kind=kOutput, calls=%fused_computation.9.clone.1 | convolution fusion | flops 271450112 | bytes 3936261 | tf_op jit(solution)/shard_map/cond/branch_1_fun/while/body/eval_jaxpr/hmqk,khe->hmqe/dot_general | solution.py:115
  184.2 0.6 fusion.76
  184.9 1.2 dynamic_slice.33
  186.8 1.1 constant_dynamic-slice_fusion.2
  188.7 2.9 %fusion.77 = f32[1,2,256,256]{3,2,1,0:T(8,128)} fusion(f32[2,1024,256]{2,1,0:T(8,128)S(1)} %get-tuple-element.243, f32[2,256]{1,0:T(2,128)S(1)} %bitcast.177, pred[256,1024]{0,1:T(8,128)(4,1)S(1)} %broadcast_compare_fusion.2, f32[1,2,256,256]{3,2,1,0:T(8,128)} %get-tuple-element.261, bf16[8192,256]{1,0:T(8,128)(2,1)} %get-tuple-element.279, ...), kind=kOutput, calls=%fused_computation.9.clone.1 | convolution fusion | flops 271450112 | bytes 3936261 | tf_op jit(solution)/shard_map/cond/branch_1_fun/while/body/eval_jaxpr/hmqk,khe->hmqe/dot_general | solution.py:115
  191.5 0.6 fusion.76
  192.2 1.2 dynamic_slice.33
  194.1 1.1 constant_dynamic-slice_fusion.2
  196.0 2.9 %fusion.77 = f32[1,2,256,256]{3,2,1,0:T(8,128)} fusion(f32[2,1024,256]{2,1,0:T(8,128)S(1)} %get-tuple-element.243, f32[2,256]{1,0:T(2,128)S(1)} %bitcast.177, pred[256,1024]{0,1:T(8,128)(4,1)S(1)} %broadcast_compare_fusion.2, f32[1,2,256,256]{3,2,1,0:T(8,128)} %get-tuple-element.261, bf16[8192,256]{1,0:T(8,128)(2,1)} %get-tuple-element.279, ...), kind=kOutput, calls=%fused_computation.9.clone.1 | convolution fusion | flops 271450112 | bytes 3936261 | tf_op jit(solution)/shard_map/cond/branch_1_fun/while/body/eval_jaxpr/hmqk,khe->hmqe/dot_general | solution.py:115
  199.5 1.2 dynamic_slice.33
  201.4 1.1 constant_dynamic-slice_fusion.2
  203.3 2.9 %fusion.77 = f32[1,2,256,256]{3,2,1,0:T(8,128)} fusion(f32[2,1024,256]{2,1,0:T(8,128)S(1)} %get-tuple-element.243, f32[2,256]{1,0:T(2,128)S(1)} %bitcast.177, pred[256,1024]{0,1:T(8,128)(4,1)S(1)} %broadcast_compare_fusion.2, f32[1,2,256,256]{3,2,1,0:T(8,128)} %get-tuple-element.261, bf16[8192,256]{1,0:T(8,128)(2,1)} %get-tuple-element.279, ...), kind=kOutput, calls=%fused_computation.9.clone.1 | convolution fusion | flops 271450112 | bytes 3936261 | tf_op jit(solution)/shard_map/cond/branch_1_fun/while/body/eval_jaxpr/hmqk,khe->hmqe/dot_general | solution.py:115
  206.8 1.9 fusion.60
  209.3 1.3 fusion.43
  210.5 2.0 fusion.25
  212.5 1.3 copy.100
  213.8 3.7 %all-to-all-start = ((bf16[16,256,128]{2,1,0:T(8,128)(2,1)}), bf16[16,256,128]{2,1,0:T(8,128)(2,1)S(1)}, u32[]{:S(2)}, u32[]{:S(2)}) async-start(bf16[16,256,128]{2,1,0:T(8,128)(2,1)} %bitcast.143), calls=%async_computation | async-start | bytes 2097152 | tf_op jit(solution)/shard_map/all_to_all | solution.py:27
  217.6 0.9 copy.73
  218.5 1.6 gather_fusion.1
  220.1 0.9 fusion.46
  221.0 14.8 %all-to-all-done = bf16[16,256,128]{2,1,0:T(8,128)(2,1)S(1)} async-done(((bf16[16,256,128]{2,1,0:T(8,128)(2,1)}), bf16[16,256,128]{2,1,0:T(8,128)(2,1)S(1)}, u32[]{:S(2)}, u32[]{:S(2)}) %all-to-all-start) | async-done | bytes 1048608 | tf_op jit(solution)/shard_map/all_to_all | solution.py:27
  235.8 0.8 reduce_sum.74
  (144 shorter events, 13.2 us)
Async XLA Ops:
  7.2 84.2 %copy-start = (bf16[1,256,2048]{2,1,0:T(8,128)(2,1)S(1)}, bf16[1,256,2048]{2,1,0:T(8,128)(2,1)}, u32[]{:S(2)}) copy-start(bf16[1,256,2048]{2,1,0:T(8,128)(2,1)} %param.29) | copy-start | bytes 3145732
  7.2 4.5 %copy-start.5 = (s32[128,2]{0,1:T(2,128)S(1)}, s32[128,2]{0,1:T(2,128)}, u32[]{:S(2)}) copy-start(s32[128,2]{0,1:T(2,128)} %param.25) | copy-start | bytes 3076
  7.2 5.0 %copy-start.2 = (bf16[128,2048]{1,0:T(8,128)(2,1)S(1)}, bf16[128,2048]{1,0:T(8,128)(2,1)}, u32[]{:S(2)}) copy-start(bf16[128,2048]{1,0:T(8,128)(2,1)} %param.23) | copy-start | bytes 1572868
  7.2 120.3 %all-gather.2.cloned.1.call-start = ((), (), s32[]{:S(2)}) async-start(), calls=%async_computation.5 | async-start | bytes 8650752 | tf_op jit(solution)/shard_map/all_gather | solution.py:12
  88.4 1.2 copy-start.9
  89.4 1.3 copy-start.10
  93.6 25.4 %all-to-all-start.3 = ((bf16[16,32,12,128]{3,1,2,0:T(8,128)(2,1)}), bf16[16,32,12,128]{3,1,2,0:T(8,128)(2,1)S(1)}, u32[]{:S(2)}, u32[]{:S(2)}) async-start(bf16[16,32,12,128]{3,1,2,0:T(8,128)(2,1)} %bitcast.173), calls=%async_computation.3 | async-start | bytes 3145728 | tf_op jit(solution)/shard_map/all_to_all | solution.py:27
  119.9 93.9 %all-to-all-start.4 = ((bf16[32,12,128]{2,1,0:T(8,128)(2,1)}), bf16[32,12,128]{2,1,0:T(8,128)(2,1)}, u32[]{:S(2)}, u32[]{:S(2)}) async-start(bf16[32,12,128]{2,1,0:T(8,128)(2,1)} %copy.72), calls=%async_computation.4 | async-start | bytes 262144 | tf_op jit(solution)/shard_map/all_to_all | solution.py:190
  139.4 6.2 %copy-start.1 = (bf16[8192,512]{0,1:T(8,128)(2,1)S(1)}, bf16[8192,512]{0,1:T(8,128)(2,1)}, u32[]{:S(2)}) copy-start(bf16[8192,512]{0,1:T(8,128)(2,1)} %get-tuple-element.138) | copy-start | bytes 25165828 | tf_op jit(solution)/shard_map/cond
  148.6 3.2 %copy-start.3 = (s32[256]{0:T(256)}, s32[256]{0:T(256)S(1)}, u32[]{:S(2)}) copy-start(s32[256]{0:T(256)S(1)} %get-tuple-element.276) | copy-start | bytes 3076 | tf_op jit(solution)/shard_map/cond/branch_1_fun/while
  155.0 0.7 copy-start.4
  155.7 3.2 %copy-start.3 = (s32[256]{0:T(256)}, s32[256]{0:T(256)S(1)}, u32[]{:S(2)}) copy-start(s32[256]{0:T(256)S(1)} %get-tuple-element.276) | copy-start | bytes 3076 | tf_op jit(solution)/shard_map/cond/branch_1_fun/while
  162.3 0.7 copy-start.4
  163.0 3.2 %copy-start.3 = (s32[256]{0:T(256)}, s32[256]{0:T(256)S(1)}, u32[]{:S(2)}) copy-start(s32[256]{0:T(256)S(1)} %get-tuple-element.276) | copy-start | bytes 3076 | tf_op jit(solution)/shard_map/cond/branch_1_fun/while
  169.6 0.7 copy-start.4
  170.3 3.2 %copy-start.3 = (s32[256]{0:T(256)}, s32[256]{0:T(256)S(1)}, u32[]{:S(2)}) copy-start(s32[256]{0:T(256)S(1)} %get-tuple-element.276) | copy-start | bytes 3076 | tf_op jit(solution)/shard_map/cond/branch_1_fun/while
  176.9 0.7 copy-start.4
  177.6 3.2 %copy-start.3 = (s32[256]{0:T(256)}, s32[256]{0:T(256)S(1)}, u32[]{:S(2)}) copy-start(s32[256]{0:T(256)S(1)} %get-tuple-element.276) | copy-start | bytes 3076 | tf_op jit(solution)/shard_map/cond/branch_1_fun/while
  184.2 0.7 copy-start.4
  184.9 3.2 %copy-start.3 = (s32[256]{0:T(256)}, s32[256]{0:T(256)S(1)}, u32[]{:S(2)}) copy-start(s32[256]{0:T(256)S(1)} %get-tuple-element.276) | copy-start | bytes 3076 | tf_op jit(solution)/shard_map/cond/branch_1_fun/while
  191.5 0.7 copy-start.4
  192.2 3.2 %copy-start.3 = (s32[256]{0:T(256)}, s32[256]{0:T(256)S(1)}, u32[]{:S(2)}) copy-start(s32[256]{0:T(256)S(1)} %get-tuple-element.276) | copy-start | bytes 3076 | tf_op jit(solution)/shard_map/cond/branch_1_fun/while
  198.8 0.7 copy-start.4
  199.5 3.2 %copy-start.3 = (s32[256]{0:T(256)}, s32[256]{0:T(256)S(1)}, u32[]{:S(2)}) copy-start(s32[256]{0:T(256)S(1)} %get-tuple-element.276) | copy-start | bytes 3076 | tf_op jit(solution)/shard_map/cond/branch_1_fun/while
  206.1 0.7 copy-start.4
  208.7 0.6 copy-start.7
  208.7 0.6 copy-start.8
  212.5 4.9 %copy-start.6 = (f32[128,2]{0,1:T(2,128)S(1)}, f32[128,2]{0,1:T(2,128)}, u32[]{:S(2)}) copy-start(f32[128,2]{0,1:T(2,128)} %param.26) | copy-start | bytes 3076
  213.8 22.0 %all-to-all-start = ((bf16[16,256,128]{2,1,0:T(8,128)(2,1)}), bf16[16,256,128]{2,1,0:T(8,128)(2,1)S(1)}, u32[]{:S(2)}, u32[]{:S(2)}) async-start(bf16[16,256,128]{2,1,0:T(8,128)(2,1)} %bitcast.143), calls=%async_computation | async-start | bytes 2097152 | tf_op jit(solution)/shard_map/all_to_all | solution.py:27
Sparse Core Ops, SparseCore 0:
  11.8 103.7 all-gather.1
where the time goes:
time: 245 us; the launch traced here: 243 us
  local copies, waits for them, and re-layouts  68.8 us (28%)
  blocking collectives  60.5 us (25%)
  waiting for transfers between devices  35.9 us (15%)
  matrix products  30.9 us (13%)
  starting transfers between devices  15 us (6%)
  between operations  15 us (6%)
  other arithmetic  11.9 us (5%)
  loops' own time  5.52 us (2%)
    all_to_all x2, waiting for transfers between devices, sum_at_owner(): lax.all_to_all(parts, axis, split_axis=0, concat_axis=0, tiled=True)  35.8 us
    all_to_all x1, blocking collectives, expert_half(): lax.all_to_all(empty.at[expert_ids, slot_index].set(sent[source_row]), 'e...  31.1 us
    all_to_all x1, blocking collectives, copy_for_each(): lax.all_to_all(jnp.broadcast_to(shard[None], (peers, *shard.shape)), axis...  29.5 us
    dot_general x8, matrix products, fold_step(): jnp.einsum('hmqk,khe->hmqe', expd.astype(jnp.bfloat16), block_v, preferre...  22.8 us
    scatter x2, local copies, waits for them, and re-layouts, expert_half(): empty.at[expert_ids, slot_index].set(sent[source_row])  12.3 us
    another operation x3, local copies, waits for them, and re-layouts  12.1 us
    dynamic_slice x8, local copies, waits for them, and re-layouts, attend(): lax.scan(fold_step, state, jnp.arange(piece_len // block_size, dtype=jnp....  9.82 us
    dynamic_slice x8, local copies, waits for them, and re-layouts, fold_step(): lax.dynamic_slice_in_dim(piece_k, block_start, block_size, 0)  8.65 us
  transfers between devices with their start and end apart: 4, of which 2 were waited for; matrix products, arithmetic and copies ran while one was open for 42% of the time, Pallas kernels for 0%

commit v1 on v0

v1 whole, which is shorter than its diff:
```python
import functools

import jax
import jax.numpy as jnp
from jax import lax
from jax.experimental import pallas as pl
from jax.experimental.pallas import tpu as pltpu
from jax.sharding import PartitionSpec as P

norm_eps = 1e-06
rope_base = 10000.0
log2e = 1.4426950408889634

NZ = 16
NX = 4
NY = 4
SLOTS = 12
PAIR = 2 * SLOTS
HALF = NZ // 2
ROWS = 256
COLS = 128

MESH = pl.DeviceIdType.MESH
bf16 = jnp.bfloat16
f32 = jnp.float32


def rope_turn(inputs, positions):
    half_dim = inputs.shape[-1] // 2
    inverse = rope_base ** (-2.0 * jnp.arange(half_dim, dtype=jnp.float32) / inputs.shape[-1])
    angles = positions.astype(jnp.float32)[:, None] * inverse[None, :]
    cos_table = jnp.cos(angles)[:, None, :]
    sin_table = jnp.sin(angles)[:, None, :]
    first_half = inputs[..., :half_dim]
    second_half = inputs[..., half_dim:]
    return jnp.concatenate(
        [
            first_half * cos_table - second_half * sin_table,
            second_half * cos_table + first_half * sin_table,
        ],
        axis=-1,
    )


def layer_kernel(
    q_t, kv_own, lam, gain, wout_hbm, disp, gate_hbm, up_hbm, down_hbm, pick0, pick1, rweights,
    mixed, expert_out,
    kv, acc, run_max, run_sum, wout, gate_w, up_w, down_w,
    exch_in, z_send, z_in, ag_a, ag_b, rs_a, rs_b, rs_a_in, rs_b_in, mid_a, mid_b, fin_a, fin_b,
    ret_send, ret, at_a, at_b, at_a_in, at_b_in, atm_a, atm_b, atf_a, atf_b,
    kv_recv, plus_send, minus_send, d2d_plus, d2d_minus, pair_send, pair_recv,
    z_sends, z_recvs, ret_sends, ret_recvs, plane_send, plane_recv, local_sem,
):
    ep = lax.axis_index("ep")
    tp = lax.axis_index("tp")
    z = ep // 2
    c = ep % 2
    y = tp // NX
    x = tp % NX
    partner = (z * 2 + 1 - c, tp)
    right = (((z + 1) % NZ) * 2 + c, tp)
    left = (((z + NZ - 1) % NZ) * 2 + c, tp)

    def z_peer(d):
        return (((z + d) % NZ) * 2 + c, tp)

    def x_peer(d):
        return (ep, y * NX + (x + d) % NX)

    def y_peer(d):
        return (ep, ((y + d) % NY) * NX + x)

    def remote(src, dst, send, recv, device):
        return pltpu.make_async_remote_copy(
            src_ref=src, dst_ref=dst, send_sem=send, recv_sem=recv,
            device_id=device, device_id_type=MESH,
        )

    loads = [
        pltpu.make_async_copy(gate_hbm, gate_w, local_sem.at[0]),
        pltpu.make_async_copy(up_hbm, up_w, local_sem.at[1]),
        pltpu.make_async_copy(down_hbm, down_w, local_sem.at[2]),
        pltpu.make_async_copy(wout_hbm, wout, local_sem.at[3]),
    ]

    barrier = pltpu.get_barrier_semaphore()
    for d in range(1, NZ):
        pl.semaphore_signal(barrier, inc=1, device_id=z_peer(d), device_id_type=MESH)
    pl.semaphore_signal(barrier, inc=1, device_id=partner, device_id_type=MESH)
    for d in range(1, 4):
        pl.semaphore_signal(barrier, inc=1, device_id=x_peer(d), device_id_type=MESH)
        pl.semaphore_signal(barrier, inc=1, device_id=y_peer(d), device_id_type=MESH)
    for load in loads:
        load.start()
    pl.semaphore_wait(barrier, NZ - 1 + 1 + 6)

    exch = remote(disp.at[1 - c], exch_in, pair_send.at[0], pair_recv.at[0], partner)
    exch.start()

    def kv_wait(slot, p):
        remote(
            kv.at[slot, p], kv.at[slot, p], plus_send.at[0, p], kv_recv.at[slot, p], left
        ).wait_recv()

    def kv_copy(src, slot, p, send, device):
        return remote(src, kv.at[slot, p], send, kv_recv.at[slot, p], device)

    exch.wait_recv()
    z_send[...] = (disp[c].astype(f32) + exch_in[...].astype(f32)).astype(bf16)
    z_in[z] = z_send[z]
    for d in range(1, NZ):
        remote(
            z_send.at[(z + d) % NZ], z_in.at[z], z_sends.at[d], z_recvs.at[d], z_peer(d)
        ).start()

    for p in range(2):
        @pl.when(z < NZ - 1)
        def _():
            kv_copy(kv_own.at[p], ep, p, plus_send.at[0, p], right).start()

        @pl.when(z <= 6 + p)
        def _():
            kv_copy(kv_own.at[p], ep, p, minus_send.at[0, p], left).start()

        @pl.when(c == 0)
        def _():
            kv_copy(kv_own.at[p], ep, p, d2d_plus.at[0, p], partner).start()

    scale = (128 ** -0.5) * log2e

    def fold(k_of, v_of, count, masked, first):
        for m in range(2):
            q_m = q_t[m * 128:(m + 1) * 128, :]
            scores = []
            for i in range(count):
                s = jnp.dot(k_of(i)[:, m * 128:(m + 1) * 128], q_m, preferred_element_type=f32)
                if masked:
                    rows = lax.broadcasted_iota(jnp.int32, s.shape, 0)
                    cols = lax.broadcasted_iota(jnp.int32, s.shape, 1)
                    s = jnp.where(rows <= cols, s, -1e30)
                scores.append(s)
            top = jnp.max(scores[0], axis=0, keepdims=True)
            for s in scores[1:]:
                top = jnp.maximum(top, jnp.max(s, axis=0, keepdims=True))
            top = top * scale
            if first:
                new_max = top
            else:
                old = run_max[m]
                new_max = jnp.maximum(old, top)
                alpha = jnp.exp2(old - new_max)
            total = None
            out = None
            for i in range(count):
                e = jnp.exp2(scores[i] * scale - new_max)
                t = jnp.sum(e, axis=0, keepdims=True)
                total = t if total is None else total + t
                o = jnp.dot(v_of(i), e.astype(bf16), preferred_element_type=f32)
                out = o if out is None else out + o
            run_max[m] = new_max
            if first:
                run_sum[m] = total
                acc[m] = out
            else:
                run_sum[m] = run_sum[m] * alpha + total
                acc[m] = acc[m] * alpha + out

    fold(lambda i: kv_own[0], lambda i: kv_own[1], 1, True, True)

    @pl.when(c == 1)
    def _():
        kv_wait(ep - 1, 0)
        kv_wait(ep - 1, 1)
        fold(lambda i: kv[ep - 1, 0], lambda i: kv[ep - 1, 1], 1, False, False)

    def fold_chip(chip):
        other = chip * 2 + 1 - c
        kv_wait(other, 0)
        kv_wait(other, 1)
        fold(
            lambda i: kv[chip * 2 + i, 0], lambda i: kv[chip * 2 + i, 1], 2, False, False
        )

    def plane_copies(index, half, src_of, dst_of, peer):
        return [
            remote(
                src_of(d), dst_of(d), plane_send.at[index, half, d - 1],
                plane_recv.at[index, half, d - 1], peer(d),
            )
            for d in range(1, 4)
        ]

    def start_all(copies):
        for cp in copies:
            cp.start()

    def wait_recvs(copies):
        for cp in copies:
            cp.wait_recv()

    def wait_sends(copies):
        for cp in copies:
            cp.wait_send()

    ag1_a = plane_copies(0, 0, lambda d: z_in.at[pl.ds(0, HALF)], lambda d: ag_a.at[y, x], x_peer)
    ag1_b = plane_copies(0, 1, lambda d: z_in.at[pl.ds(HALF, HALF)], lambda d: ag_b.at[x, y], y_peer)
    ag2_a = plane_copies(1, 0, lambda d: ag_a.at[y], lambda d: ag_a.at[y], y_peer)
    ag2_b = plane_copies(1, 1, lambda d: ag_b.at[x], lambda d: ag_b.at[x], x_peer)
    rs1_a = plane_copies(2, 0, lambda d: rs_a.at[(y + d) % NY], lambda d: rs_a_in.at[d - 1], y_peer)
    rs1_b = plane_copies(2, 1, lambda d: rs_b.at[(x + d) % NX], lambda d: rs_b_in.at[d - 1], x_peer)
    rs2_a = plane_copies(3, 0, lambda d: mid_a.at[(x + d) % NX], lambda d: fin_a.at[d - 1], x_peer)
    rs2_b = plane_copies(3, 1, lambda d: mid_b.at[(y + d) % NY], lambda d: fin_b.at[d - 1], y_peer)
    at1_a = plane_copies(4, 0, lambda d: at_a.at[(y + d) % NY], lambda d: at_a_in.at[d - 1], y_peer)
    at1_b = plane_copies(4, 1, lambda d: at_b.at[(x + d) % NX], lambda d: at_b_in.at[d - 1], x_peer)
    at2_a = plane_copies(5, 0, lambda d: atm_a.at[(x + d) % NX], lambda d: atf_a.at[d - 1], x_peer)
    at2_b = plane_copies(5, 1, lambda d: atm_b.at[(y + d) % NY], lambda d: atf_b.at[d - 1], y_peer)

    def gather_one():
        for d in range(1, NZ):
            remote(
                z_send.at[d], z_in.at[(z + NZ - d) % NZ], z_sends.at[d], z_recvs.at[d], z_peer(d)
            ).wait_recv()
        ag_a[y, x] = z_in[0:HALF]
        ag_b[x, y] = z_in[HALF:NZ]
        start_all(ag1_a)
        start_all(ag1_b)

    def gather_two():
        for d in range(1, 4):
            remote(
                ag_a.at[y, x], ag_a.at[y, (x + 4 - d) % NX], plane_send.at[0, 0, d - 1],
                plane_recv.at[0, 0, d - 1], x_peer(d),
            ).wait_recv()
            remote(
                ag_b.at[x, y], ag_b.at[x, (y + 4 - d) % NY], plane_send.at[0, 1, d - 1],
                plane_recv.at[0, 1, d - 1], y_peer(d),
            ).wait_recv()
        start_all(ag2_a)
        start_all(ag2_b)

    def expert(half):
        if half == 0:
            for load in loads[:3]:
                load.wait()
        for d in range(1, 4):
            if half == 0:
                remote(
                    ag_a.at[y], ag_a.at[(y + 4 - d) % NY], plane_send.at[1, 0, d - 1],
                    plane_recv.at[1, 0, d - 1], y_peer(d),
                ).wait_recv()
            else:
                remote(
                    ag_b.at[x], ag_b.at[(x + 4 - d) % NX], plane_send.at[1, 1, d - 1],
                    plane_recv.at[1, 1, d - 1], x_peer(d),
                ).wait_recv()
        n = HALF * PAIR
        pieces = [
            (ag_a[i, j] if half == 0 else ag_b[j, i]).reshape(n, COLS)
            for i in range(NY)
            for j in range(NX)
        ]
        rows = jnp.concatenate(pieces, axis=1)
        g = jnp.dot(rows, gate_w[...], preferred_element_type=f32)
        u = jnp.dot(rows, up_w[...], preferred_element_type=f32)
        hidden = (g / (1.0 + jnp.exp(-g)) * u).astype(bf16)
        for i in range(NY):
            for j in range(NX):
                at = (i * NX + j) * COLS
                part = jnp.dot(
                    hidden, down_w[:, at:at + COLS], preferred_element_type=f32
                ).astype(bf16)
                if half == 0:
                    rs_a[i, j] = part
                else:
                    rs_b[j, i] = part
        start_all(rs1_a if half == 0 else rs1_b)

    def sum_one():
        wait_recvs(rs1_a)
        for j in range(4):
            t = rs_a[y, j].astype(f32)
            for d in range(3):
                t = t + rs_a_in[d, j].astype(f32)
            mid_a[j] = t.astype(bf16)
        start_all(rs2_a)
        wait_recvs(rs1_b)
        for j in range(4):
            t = rs_b[x, j].astype(f32)
            for d in range(3):
                t = t + rs_b_in[d, j].astype(f32)
            mid_b[j] = t.astype(bf16)
        start_all(rs2_b)

    def sum_two():
        wait_recvs(rs2_a)
        wait_recvs(rs2_b)
        t = mid_a[x].astype(f32)
        for d in range(3):
            t = t + fin_a[d].astype(f32)
        ret_send[0:HALF] = t.astype(bf16).reshape(HALF, PAIR, COLS)
        t = mid_b[y].astype(f32)
        for d in range(3):
            t = t + fin_b[d].astype(f32)
        ret_send[HALF:NZ] = t.astype(bf16).reshape(HALF, PAIR, COLS)
        ret[0, z] = ret_send[z]
        for d in range(1, NZ):
            remote(
                ret_send.at[(z + d) % NZ], ret.at[0, z], ret_sends.at[d], ret_recvs.at[d],
                z_peer(d),
            ).start()

    def tick(s, carry):
        zl = jnp.maximum(z - s, 0)
        zr = (z + s) % NZ
        wrapped = z + s >= NZ

        def plus(p, last):
            @pl.when((s <= last) & (s <= z))
            def _():
                slot = zl * 2 + c
                kv_wait(slot, p)

                @pl.when((z < NZ - 1) & (s < last))
                def _():
                    kv_copy(kv.at[slot, p], slot, p, plus_send.at[s, p], right).start()

                kv_copy(kv.at[slot, p], slot, p, d2d_plus.at[s, p], partner).start()

        def minus(p, last):
            @pl.when((s <= last) & (zr <= 6 + p))
            def _():
                slot = zr * 2 + c
                kv_wait(slot, p)

                @pl.when(s < last)
                def _():
                    kv_copy(kv.at[slot, p], slot, p, minus_send.at[s, p], left).start()

                @pl.when(wrapped)
                def _():
                    kv_copy(kv.at[slot, p], slot, p, d2d_minus.at[s, p], partner).start()

        plus(0, 8)
        minus(0, 7)

        @pl.when(s == 2)
        def _():
            gather_one()

        @pl.when(s == 3)
        def _():
            gather_two()

        @pl.when((s >= 2) & (s - 1 <= z))
        def _():
            fold_chip(jnp.maximum(z - s + 1, 0))

        plus(1, 7)
        minus(1, 8)

        @pl.when(s == 5)
        def _():
            expert(0)

        @pl.when(s == 6)
        def _():
            expert(1)

        @pl.when(s == 7)
        def _():
            sum_one()

        @pl.when(s == 8)
        def _():
            sum_two()

        @pl.when((s >= 2) & (s - 1 <= 7) & (z + s - 1 >= NZ))
        def _():
            fold_chip(jnp.maximum(z + s - 1 - NZ, 0))

        return carry

    lax.fori_loop(1, 10, tick, 0)

    first = acc[0] / run_sum[0]
    second = acc[1] / run_sum[1]
    diff = first - lam[0, 0] * second
    mean = jnp.mean(diff * diff, axis=0, keepdims=True)
    head_t = diff * lax.rsqrt(mean + norm_eps) * gain[...]
    head = head_t.T.astype(bf16)
    loads[3].wait()
    for i in range(NY):
        for j in range(NX):
            at = (i * NX + j) * COLS
            part = jnp.dot(head, wout[:, at:at + COLS], preferred_element_type=f32).astype(bf16)
            at_a[i, j] = part[:ROWS // 2]
            at_b[j, i] = part[ROWS // 2:]
    start_all(at1_a)
    start_all(at1_b)

    for d in range(1, NZ):
        remote(
            ret_send.at[d], ret.at[0, (z + NZ - d) % NZ], ret_sends.at[d], ret_recvs.at[d],
            z_peer(d),
        ).wait_recv()
    back = remote(ret.at[0], ret.at[1], pair_send.at[1], pair_recv.at[1], partner)
    back.start()

    wait_recvs(at1_a)
    for j in range(4):
        t = at_a[y, j].astype(f32)
        for d in range(3):
            t = t + at_a_in[d, j].astype(f32)
        atm_a[j] = t.astype(bf16)
    start_all(at2_a)
    wait_recvs(at1_b)
    for j in range(4):
        t = at_b[x, j].astype(f32)
        for d in range(3):
            t = t + at_b_in[d, j].astype(f32)
        atm_b[j] = t.astype(bf16)
    start_all(at2_b)

    back.wait_recv()
    rows = ret[...].reshape(2 * NZ * PAIR, COLS)
    chosen = jnp.dot(pick0[...], rows, preferred_element_type=f32) * rweights[:, 0:1]
    chosen = chosen + jnp.dot(pick1[...], rows, preferred_element_type=f32) * rweights[:, 1:2]
    expert_out[...] = chosen.astype(bf16)

    wait_recvs(at2_a)
    t = atm_a[x].astype(f32)
    for d in range(3):
        t = t + atf_a[d].astype(f32)
    mixed[0:ROWS // 2] = t.astype(bf16)
    wait_recvs(at2_b)
    t = atm_b[y].astype(f32)
    for d in range(3):
        t = t + atf_b[d].astype(f32)
    mixed[ROWS // 2:ROWS] = t.astype(bf16)

    exch.wait_send()
    back.wait_send()
    for d in range(1, NZ):
        remote(
            z_send.at[d], z_in.at[d], z_sends.at[d], z_recvs.at[d], z_peer(d)
        ).wait_send()
        remote(
            ret_send.at[d], ret.at[0, d], ret_sends.at[d], ret_recvs.at[d], z_peer(d)
        ).wait_send()
    for copies in (
        ag1_a, ag1_b, ag2_a, ag2_b, rs1_a, rs1_b, rs2_a, rs2_b, at1_a, at1_b, at2_a, at2_b
    ):
        wait_sends(copies)

    def sent(sem, p):
        remote(kv_own.at[p], kv.at[0, p], sem, kv_recv.at[0, p], left).wait_send()

    for p in range(2):
        @pl.when(z < NZ - 1)
        def _():
            sent(plus_send.at[0, p], p)

        @pl.when(z <= 6 + p)
        def _():
            sent(minus_send.at[0, p], p)

        @pl.when(c == 0)
        def _():
            sent(d2d_plus.at[0, p], p)

    def drain(s, carry):
        zr = (z + s) % NZ
        for p in range(2):
            last_p, last_m = 8 - p, 7 + p

            @pl.when((s <= last_p) & (s <= z))
            def _():
                @pl.when((z < NZ - 1) & (s < last_p))
                def _():
                    sent(plus_send.at[s, p], p)

                sent(d2d_plus.at[s, p], p)

            @pl.when((s <= last_m) & (zr <= 6 + p))
            def _():
                @pl.when(s < last_m)
                def _():
                    sent(minus_send.at[s, p], p)

                @pl.when(z + s >= NZ)
                def _():
                    sent(d2d_minus.at[s, p], p)

        return carry

    lax.fori_loop(1, 9, drain, 0)


def call_kernel(*operands):
    vmem = pl.BlockSpec(memory_space=pltpu.VMEM)
    hbm = pl.BlockSpec(memory_space=pl.ANY)
    smem = pl.BlockSpec(memory_space=pltpu.SMEM)
    n = HALF * PAIR
    h = ROWS // 2
    V = lambda *shape: pltpu.VMEM(shape, bf16)
    D = lambda *shape: pltpu.SemaphoreType.DMA(shape)
    return pl.pallas_call(
        layer_kernel,
        out_shape=(
            jax.ShapeDtypeStruct((ROWS, COLS), bf16),
            jax.ShapeDtypeStruct((128, COLS), bf16),
        ),
        in_specs=[vmem, vmem, smem, vmem, hbm, vmem, hbm, hbm, hbm, vmem, vmem, vmem],
        out_specs=(vmem, vmem),
        scratch_shapes=[
            V(2 * NZ, 2, ROWS, ROWS),
            pltpu.VMEM((2, ROWS, ROWS), f32),
            pltpu.VMEM((2, 1, ROWS), f32),
            pltpu.VMEM((2, 1, ROWS), f32),
            V(ROWS, 2048), V(2048, 256), V(2048, 256), V(256, 2048),
            V(NZ, PAIR, COLS), V(NZ, PAIR, COLS), V(NZ, PAIR, COLS),
            V(4, 4, HALF, PAIR, COLS), V(4, 4, HALF, PAIR, COLS),
            V(4, 4, n, COLS), V(4, 4, n, COLS), V(3, 4, n, COLS), V(3, 4, n, COLS),
            V(4, n, COLS), V(4, n, COLS), V(3, n, COLS), V(3, n, COLS),
            V(NZ, PAIR, COLS), V(2, NZ, PAIR, COLS),
            V(4, 4, h, COLS), V(4, 4, h, COLS), V(3, 4, h, COLS), V(3, 4, h, COLS),
            V(4, h, COLS), V(4, h, COLS), V(3, h, COLS), V(3, h, COLS),
            D(32, 2), D(8, 2), D(8, 2), D(9, 2), D(9, 2), D(2), D(2),
            D(NZ), D(NZ), D(NZ), D(NZ), D(6, 2, 3), D(6, 2, 3), D(4),
        ],
        compiler_params=pltpu.CompilerParams(
            collective_id=0, has_side_effects=True, vmem_limit_bytes=60 * 1024 * 1024
        ),
    )(*operands)


def on_device(
    query_maps, key_maps, value_rows, head_lambda, head_gain, out_weight,
    expert_rows, expert_gain, routes, route_weights, gate_weight, up_weight, down_weight,
):
    ep = lax.axis_index("ep")
    tp = lax.axis_index("tp")
    core = ep % 2
    row_count = query_maps.shape[0]
    positions = ep * row_count + jnp.arange(row_count, dtype=jnp.int32)

    def turned(maps):
        wide = maps.astype(f32).reshape(row_count, 2, 128)
        return rope_turn(wide, positions).astype(bf16).reshape(row_count, 256)

    q_t = turned(query_maps).T
    kv_own = jnp.stack([turned(key_maps), value_rows.T])

    inputs = expert_rows.astype(f32)
    normed = (
        inputs
        * lax.rsqrt(jnp.mean(inputs * inputs, axis=-1, keepdims=True) + norm_eps)
        * expert_gain
    ).astype(bf16)
    mine = lax.dynamic_slice_in_dim(normed, tp * COLS, COLS, 1)
    tokens, picks = routes.shape
    ids = routes.reshape(-1)
    one_hot = (ids[:, None] == jnp.arange(32, dtype=jnp.int32)[None, :]).astype(f32)
    order = jnp.arange(tokens * picks, dtype=jnp.int32)
    before = (order[None, :] < order[:, None]).astype(bf16)
    counts = jnp.dot(before, one_hot.astype(bf16), preferred_element_type=f32)
    slot = jnp.sum(counts * one_hot, axis=1).astype(jnp.int32).reshape(tokens, picks)
    base = (routes // 2) * PAIR + core * SLOTS + slot
    to_row = (routes % 2) * (NZ * PAIR) + base
    from_row = (routes % 2 != core).astype(jnp.int32) * (NZ * PAIR) + base
    lines = jnp.arange(2 * NZ * PAIR, dtype=jnp.int32)
    place = (lines[:, None] == to_row[None, :, 0]) | (lines[:, None] == to_row[None, :, 1])
    disp = jnp.dot(place.astype(bf16), mine, preferred_element_type=f32).astype(bf16)
    disp = disp.reshape(2, NZ, PAIR, COLS)
    pick0 = (from_row[:, 0:1] == lines[None, :]).astype(bf16)
    pick1 = (from_row[:, 1:2] == lines[None, :]).astype(bf16)

    return call_kernel(
        q_t, kv_own, head_lambda.reshape(1, 1), head_gain.reshape(-1, 1), out_weight,
        disp, gate_weight[0], up_weight[0], down_weight[0], pick0, pick1, route_weights,
    )


def solution(mesh):
    placed = (
        P("ep", "tp"),
        P("ep", "tp"),
        P("ep", "tp"),
        P("tp"),
        P(),
        P("tp", None),
        P("ep", None),
        P(),
        P("ep", None),
        P("ep", None),
        P("ep", None, "tp"),
        P("ep", None, "tp"),
        P("ep", "tp", None),
    )
    return jax.shard_map(
        on_device,
        mesh=mesh,
        in_specs=placed,
        out_specs=(P("ep", "tp"), P("ep", "tp")),
        check_vma=False,
    )
```

time: 245 us -> 107 us (0.44)
  the two profiles are of different devices: /device:TPU:32 before, /device:TPU:4 now
where the time goes in v1:
time: 107 us
  Pallas kernels  91.4 us (85%)
  local copies, waits for them, and re-layouts  7.77 us (7%)
  other arithmetic  4.65 us (4%)
  between operations  1.53 us (1%)
  matrix products  1.17 us (1%)
    pallas_call x1, Pallas kernels, call_kernel(): pl.pallas_call(layer_kernel, out_shape=(jax.ShapeDtypeStruct((ROWS, COLS)...  91.4 us
    unnamed x19, local copies, waits for them, and re-layouts  3.57 us

profile of v1, /device:TPU:4, one launch (start us, length us, event | category | flops | bytes accessed | tf_op | source)
XLA Modules:
  0.0 106.5 jit_solution(16932630679116453229)
XLA Ops:
  0.6 1.0 reshape.121
  1.7 0.0 copy-start.1
  1.7 0.5 multiply_cosine_fusion
  2.2 0.4 copy-done.1
  2.6 0.1 reshape.119
  2.7 0.7 subtract_convert_fusion
  3.5 0.7 pad_maximum_fusion.1
  4.2 0.0 copy-start.2
  4.2 0.8 copy.30
  5.0 0.1 copy-done.2
  5.1 0.1 copy.31
  5.2 0.1 convert_element_type.59
  5.3 0.0 copy-start.4
  5.3 0.0 copy-start.5
  5.3 0.7 pad_maximum_fusion.kv_own
  6.1 0.0 copy-start
  6.8 0.0 copy-done.4
  6.8 0.8 copy.40.gain
  7.6 0.0 copy-done.5
  7.6 0.1 copy.36
  7.7 0.1 copy.33
  7.8 0.1 eq.81
  8.0 0.2 fusion
  8.2 0.1 convert_element_type.63
  8.4 0.1 select_add_fusion
  8.5 0.2 slice_reduce_fusion
  8.7 0.0 copy-done
  8.7 0.1 convert_element_type.64
  8.8 0.8 dynamic-slice
  9.6 0.2 multiply_reduce_fusion
  9.8 1.0 convolution_convert_fusion
  10.7 0.8 fusion.3.pick0
  11.5 0.0 copy-start.6
  11.5 0.8 fusion.4.pick1
  12.3 0.0 copy-done.6
  12.3 0.7 copy.41.rweights
  13.0 91.4 %shard_map.140 = (bf16[256,128]{1,0:T(8,128)(2,1)}, bf16[128,128]{1,0:T(8,128)(2,1)}) custom-call(bf16[256,256]{1,0:T(8,128)(2,1)} %bitcast.16, bf16[2,256,256]{2,1,0:T(8,128)(2,1)} %pad_maximum_fusion.kv_own, f32[1,1]{1,0:T(1,128)} %bitcast.12.lam, f32[256,1]{1,0:T(8,128)} %copy.40.gain, bf16[256,2048]{1,0:T(8,128)(2,1)} %wout_hbm.1, ...), custom_call_target="tpu_custom_call" | custom-call | tf_op jit(solution)/shard_map/pallas_call | solution.py:507
  104.4 0.0 copy-start.3
  104.4 1.5 %copy.50 = bf16[256,128]{1,0:T(8,128)(2,1)} copy(bf16[256,128]{1,0:T(8,128)(2,1)} %get-tuple-element.22) | data formatting | bytes 131072
  105.9 0.0 copy-done.3
  105.9 0.6 copy.51
  (5 shorter events, 0.0 us)
Async XLA Ops:
  1.7 0.9 copy-start.1
  4.2 0.9 copy-start.2
  5.3 1.5 %copy-start.4 = (f32[256]{0:T(256)S(1)}, f32[256]{0:T(256)}, u32[]{:S(2)}) copy-start(f32[256]{0:T(256)} %param.17) | copy-start | bytes 3076
  5.3 2.3 %copy-start.5 = (s32[128,2]{0,1:T(2,128)S(1)}, s32[128,2]{0,1:T(2,128)}, u32[]{:S(2)}) copy-start(s32[128,2]{0,1:T(2,128)} %param.21) | copy-start | bytes 3076
  6.1 2.6 %copy-start = (bf16[128,2048]{1,0:T(8,128)(2,1)S(1)}, bf16[128,2048]{1,0:T(8,128)(2,1)}, u32[]{:S(2)}) copy-start(bf16[128,2048]{1,0:T(8,128)(2,1)} %param.19) | copy-start | bytes 1572868
  11.5 0.8 copy-start.6
  104.4 1.5 %copy-start.3 = (bf16[128,128]{1,0:T(8,128)(2,1)S(1)}, bf16[128,128]{1,0:T(8,128)(2,1)}, u32[]{:S(2)}) copy-start(bf16[128,128]{1,0:T(8,128)(2,1)} %get-tuple-element.23) | copy-start | bytes 98308

commit v2 on v1

v2 whole, which is shorter than its diff:
```python
import functools

import jax
import jax.numpy as jnp
from jax import lax
from jax.experimental import pallas as pl
from jax.experimental.pallas import tpu as pltpu
from jax.sharding import PartitionSpec as P

norm_eps = 1e-06
rope_base = 10000.0
log2e = 1.4426950408889634

NZ = 16
NX = 4
NY = 4
SLOTS = 12
PAIR = 2 * SLOTS
HALF = NZ // 2
ROWS = 256
COLS = 128

MESH = pl.DeviceIdType.MESH
bf16 = jnp.bfloat16
f32 = jnp.float32


def layer_kernel(
    q_hbm, k_hbm, v_hbm, cos_hbm, sin_hbm, lam, gain_hbm, wout_hbm, rows_hbm, rgain_hbm,
    routes_hbm, rweights_hbm, gate_hbm, up_hbm, down_hbm,
    mixed_hbm, expert_hbm,
    q_in, k_in, v_in, cos_t, sin_t, gain, row_in, rgain, routes, rweights,
    q_t, kv_own, disp, pick, spread, mixed, expert_out,
    kv, acc, run_max, run_sum, wout, gate_w, up_w, down_w,
    exch_in, z_send, z_in, ag_a, ag_b, rs_a, rs_b, rs_a_in, rs_b_in, mid_a, mid_b, fin_a, fin_b,
    ret_send, ret, at_a, at_b, at_a_in, at_b_in, atm_a, atm_b, atf_a, atf_b,
    ring_recv, core_recv, kv_sent, pair_send, pair_recv,
    z_sent, z_came, ret_sent, ret_came, plane_send, plane_recv, local_sem,
):
    ep = lax.axis_index("ep")
    tp = lax.axis_index("tp")
    z = ep // 2
    c = ep % 2
    y = tp // NX
    x = tp % NX
    partner = (z * 2 + 1 - c, tp)
    right = (((z + 1) % NZ) * 2 + c, tp)
    left = (((z + NZ - 1) % NZ) * 2 + c, tp)

    def z_peer(d):
        return (((z + d) % NZ) * 2 + c, tp)

    def x_peer(d):
        return (ep, y * NX + (x + d) % NX)

    def y_peer(d):
        return (ep, ((y + d) % NY) * NX + x)

    def remote(src, dst, send, recv, device):
        return pltpu.make_async_remote_copy(
            src_ref=src, dst_ref=dst, send_sem=send, recv_sem=recv,
            device_id=device, device_id_type=MESH,
        )

    loads = [
        pltpu.make_async_copy(src, dst, local_sem.at[i])
        for i, (src, dst) in enumerate(
            (
                (k_hbm, k_in), (cos_hbm, cos_t), (sin_hbm, sin_t), (v_hbm, v_in),
                (rows_hbm, row_in), (routes_hbm, routes), (rgain_hbm, rgain), (q_hbm, q_in),
                (rweights_hbm, rweights), (gate_hbm, gate_w), (up_hbm, up_w),
                (down_hbm, down_w), (wout_hbm, wout), (gain_hbm, gain),
            )
        )
    ]

    barrier = pltpu.get_barrier_semaphore()
    for d in range(NZ // 2, 0, -1):
        pl.semaphore_signal(barrier, inc=1, device_id=z_peer(d), device_id_type=MESH)
        if d < NZ // 2:
            pl.semaphore_signal(barrier, inc=1, device_id=z_peer(NZ - d), device_id_type=MESH)
    for d in range(1, 4):
        pl.semaphore_signal(barrier, inc=1, device_id=x_peer(d), device_id_type=MESH)
        pl.semaphore_signal(barrier, inc=1, device_id=y_peer(d), device_id_type=MESH)
    pl.semaphore_signal(barrier, inc=1, device_id=partner, device_id_type=MESH)
    for load in loads:
        load.start()

    def turned(maps, m):
        wide = maps[:, m * 128:(m + 1) * 128].astype(f32)
        return wide * cos_t[...] + pltpu.roll(wide, 64, 1) * sin_t[...]

    for i in range(3):
        loads[i].wait()
    for m in range(2):
        kv_own[0, :, m * 128:(m + 1) * 128] = turned(k_in, m).astype(bf16)
    loads[3].wait()
    kv_own[1] = v_in[...].astype(f32).T.astype(bf16)

    for i in range(4, 7):
        loads[i].wait()
    wide = row_in[...].astype(f32)
    level = lax.rsqrt(jnp.mean(wide * wide, axis=1, keepdims=True) + norm_eps)
    column = pl.ds(pl.multiple_of(tp * COLS, COLS), COLS)
    normed = (row_in[:, column].astype(f32) * level * rgain[:, column]).astype(bf16)
    chosen = [routes[k:k + 1, :] for k in range(2)]
    names = lax.broadcasted_iota(jnp.int32, (32, 128), 0)
    hot = [(names == r).astype(f32) for r in chosen]
    earlier = (
        lax.broadcasted_iota(jnp.int32, (128, 128), 0)
        < lax.broadcasted_iota(jnp.int32, (128, 128), 1)
    )
    counts = jnp.dot(
        (hot[0] + hot[1]).astype(bf16), earlier.astype(f32).astype(bf16),
        preferred_element_type=f32,
    )
    lines = lax.broadcasted_iota(jnp.int32, (2 * NZ * PAIR, 128), 0).astype(f32)
    base = [
        ((r // 2) * PAIR + c * SLOTS).astype(f32) + jnp.sum(counts * h, axis=0, keepdims=True)
        for r, h in zip(chosen, hot)
    ]
    block = float(NZ * PAIR)
    to_row = [b + (r % 2).astype(f32) * block for b, r in zip(base, chosen)]
    from_row = [
        b + jnp.where(r % 2 == c, 0.0, block) for b, r in zip(base, chosen)
    ]
    place = jnp.where((lines == to_row[0]) | (lines == to_row[1]), 1.0, 0.0).astype(bf16)
    disp[...] = (
        jnp.dot(place, normed, preferred_element_type=f32)
        .astype(bf16)
        .reshape(2, NZ, PAIR, COLS)
    )
    pl.semaphore_wait(barrier, NZ - 1 + 1 + 6)

    exch = remote(disp.at[1 - c], exch_in, pair_send.at[0], pair_recv.at[0], partner)
    exch.start()

    def ring_piece(chip, p):
        return kv.at[chip * 4 + c * 2 + p]

    def ring_wait(chip, p):
        here = ring_piece(chip, p)
        remote(here, here, kv_sent.at[0], ring_recv.at[chip, p], left).wait_recv()

    def core_wait(chip):
        here = kv.at[pl.ds(chip * 4 + 2 - c * 2, 2)]
        remote(here, here, kv_sent.at[2], core_recv.at[chip], partner).wait_recv()

    def ring_copy(src, chip, p, way, device):
        return remote(src, ring_piece(chip, p), kv_sent.at[way], ring_recv.at[chip, p], device)

    def core_copy(src, chip, p):
        return remote(src, ring_piece(chip, p), kv_sent.at[2], core_recv.at[chip], partner)

    def send_own(p):
        @pl.when(z < NZ - 1)
        def _():
            ring_copy(kv_own.at[p], z, p, 0, right).start()

        @pl.when(z <= 6 + p)
        def _():
            ring_copy(kv_own.at[p], z, p, 1, left).start()

        @pl.when(c == 0)
        def _():
            core_copy(kv_own.at[p], z, p).start()

    send_own(0)
    exch.wait_recv()
    z_send[...] = (disp[c].astype(f32) + exch_in[...].astype(f32)).astype(bf16)
    z_in[z] = z_send[z]
    for d in range(1, NZ):
        remote(
            z_send.at[(z + d) % NZ], z_in.at[z], z_sent.at[0], z_came.at[0], z_peer(d)
        ).start()
    send_own(1)

    loads[7].wait()
    for m in range(2):
        q_t[m * 128:(m + 1) * 128, :] = turned(q_in, m).T.astype(bf16)
    loads[8].wait()
    for k in range(2):
        pick[k] = jnp.where(lines == from_row[k], 1.0, 0.0).T.astype(bf16)
        spread[k] = jnp.broadcast_to(rweights[k:k + 1, :], (128, 128)).T

    scale = (128 ** -0.5) * log2e

    def fold(k_of, v_of, count, masked, first):
        for m in range(2):
            q_m = q_t[m * 128:(m + 1) * 128, :]
            scores = []
            for i in range(count):
                s = jnp.dot(k_of(i)[:, m * 128:(m + 1) * 128], q_m, preferred_element_type=f32)
                if masked:
                    rows = lax.broadcasted_iota(jnp.int32, s.shape, 0)
                    cols = lax.broadcasted_iota(jnp.int32, s.shape, 1)
                    s = jnp.where(rows <= cols, s, -1e30)
                scores.append(s)
            top = jnp.max(scores[0], axis=0, keepdims=True)
            for s in scores[1:]:
                top = jnp.maximum(top, jnp.max(s, axis=0, keepdims=True))
            top = top * scale
            if first:
                new_max = top
            else:
                old = run_max[m]
                new_max = jnp.maximum(old, top)
                alpha = jnp.exp2(old - new_max)
            total = None
            out = None
            for i in range(count):
                e = jnp.exp2(scores[i] * scale - new_max)
                t = jnp.sum(e, axis=0, keepdims=True)
                total = t if total is None else total + t
                o = jnp.dot(v_of(i), e.astype(bf16), preferred_element_type=f32)
                out = o if out is None else out + o
            run_max[m] = new_max
            if first:
                run_sum[m] = total
                acc[m] = out
            else:
                run_sum[m] = run_sum[m] * alpha + total
                acc[m] = acc[m] * alpha + out

    fold(lambda i: kv_own[0], lambda i: kv_own[1], 1, True, True)

    @pl.when(c == 1)
    def _():
        core_wait(z)
        fold(lambda i: kv[z * 4], lambda i: kv[z * 4 + 1], 1, False, False)

    def fold_chip(chip):
        core_wait(chip)
        fold(
            lambda i: kv[chip * 4 + i * 2], lambda i: kv[chip * 4 + i * 2 + 1], 2, False, False
        )

    def plane_copies(index, half, src_of, dst_of, peer):
        return [
            remote(
                src_of(d), dst_of(d), plane_send.at[index, half],
                plane_recv.at[index, half], peer(d),
            )
            for d in range(1, 4)
        ]

    def start_all(copies):
        for cp in copies:
            cp.start()

    def three(index, half, ref):
        return remote(
            ref, ref, plane_send.at[index, half], plane_recv.at[index, half], partner
        )

    ag1_a = plane_copies(0, 0, lambda d: z_in.at[pl.ds(0, HALF)], lambda d: ag_a.at[y, x], x_peer)
    ag1_b = plane_copies(0, 1, lambda d: z_in.at[pl.ds(HALF, HALF)], lambda d: ag_b.at[x, y], y_peer)
    ag2_a = plane_copies(1, 0, lambda d: ag_a.at[y], lambda d: ag_a.at[y], y_peer)
    ag2_b = plane_copies(1, 1, lambda d: ag_b.at[x], lambda d: ag_b.at[x], x_peer)
    rs1_a = plane_copies(2, 0, lambda d: rs_a.at[(y + d) % NY], lambda d: rs_a_in.at[d - 1], y_peer)
    rs1_b = plane_copies(2, 1, lambda d: rs_b.at[(x + d) % NX], lambda d: rs_b_in.at[d - 1], x_peer)
    rs2_a = plane_copies(3, 0, lambda d: mid_a.at[(x + d) % NX], lambda d: fin_a.at[d - 1], x_peer)
    rs2_b = plane_copies(3, 1, lambda d: mid_b.at[(y + d) % NY], lambda d: fin_b.at[d - 1], y_peer)
    at1_a = plane_copies(4, 0, lambda d: at_a.at[(y + d) % NY], lambda d: at_a_in.at[d - 1], y_peer)
    at1_b = plane_copies(4, 1, lambda d: at_b.at[(x + d) % NX], lambda d: at_b_in.at[d - 1], x_peer)
    at2_a = plane_copies(5, 0, lambda d: atm_a.at[(x + d) % NX], lambda d: atf_a.at[d - 1], x_peer)
    at2_b = plane_copies(5, 1, lambda d: atm_b.at[(y + d) % NY], lambda d: atf_b.at[d - 1], y_peer)

    def gather_one():
        most = pl.ds(0, NZ - 1)
        remote(
            z_send.at[most], z_in.at[most], z_sent.at[0], z_came.at[0], partner
        ).wait_recv()
        ag_a[y, x] = z_in[0:HALF]
        ag_b[x, y] = z_in[HALF:NZ]
        start_all(ag1_a)
        start_all(ag1_b)

    def gather_two():
        three(0, 0, ag_a.at[0, pl.ds(0, 3)]).wait_recv()
        three(0, 1, ag_b.at[0, pl.ds(0, 3)]).wait_recv()
        start_all(ag2_a)
        start_all(ag2_b)

    def expert(half):
        if half == 0:
            for load in loads[9:12]:
                load.wait()
        three(1, half, (ag_b if half else ag_a).at[pl.ds(0, 3)]).wait_recv()
        n = HALF * PAIR
        pieces = [
            (ag_a[i, j] if half == 0 else ag_b[j, i]).reshape(n, COLS)
            for i in range(NY)
            for j in range(NX)
        ]
        rows = jnp.concatenate(pieces, axis=1)
        g = jnp.dot(rows, gate_w[...], preferred_element_type=f32)
        u = jnp.dot(rows, up_w[...], preferred_element_type=f32)
        hidden = (g / (1.0 + jnp.exp(-g)) * u).astype(bf16)
        for i in range(NY):
            for j in range(NX):
                at = (i * NX + j) * COLS
                part = jnp.dot(
                    hidden, down_w[:, at:at + COLS], preferred_element_type=f32
                ).astype(bf16)
                if half == 0:
                    rs_a[i, j] = part
                else:
                    rs_b[j, i] = part
        start_all(rs1_a if half == 0 else rs1_b)

    def sum_one_a():
        three(2, 0, rs_a_in).wait_recv()
        for j in range(4):
            t = rs_a[y, j].astype(f32)
            for d in range(3):
                t = t + rs_a_in[d, j].astype(f32)
            mid_a[j] = t.astype(bf16)
        start_all(rs2_a)

    def sum_one_b():
        three(2, 1, rs_b_in).wait_recv()
        for j in range(4):
            t = rs_b[x, j].astype(f32)
            for d in range(3):
                t = t + rs_b_in[d, j].astype(f32)
            mid_b[j] = t.astype(bf16)
        start_all(rs2_b)

    def sum_two():
        three(3, 0, fin_a).wait_recv()
        three(3, 1, fin_b).wait_recv()
        t = mid_a[x].astype(f32)
        for d in range(3):
            t = t + fin_a[d].astype(f32)
        ret_send[0:HALF] = t.astype(bf16).reshape(HALF, PAIR, COLS)
        t = mid_b[y].astype(f32)
        for d in range(3):
            t = t + fin_b[d].astype(f32)
        ret_send[HALF:NZ] = t.astype(bf16).reshape(HALF, PAIR, COLS)
        ret[0, z] = ret_send[z]
        for d in range(1, NZ):
            remote(
                ret_send.at[(z + d) % NZ], ret.at[0, z], ret_sent.at[0], ret_came.at[0],
                z_peer(d),
            ).start()

    def tick(s, carry):
        zl = jnp.maximum(z - s, 0)
        zr = (z + s) % NZ
        wrapped = z + s >= NZ

        def plus(p, last):
            @pl.when((s <= last) & (s <= z))
            def _():
                ring_wait(zl, p)

                @pl.when((z < NZ - 1) & (s < last))
                def _():
                    ring_copy(ring_piece(zl, p), zl, p, 0, right).start()

                core_copy(ring_piece(zl, p), zl, p).start()

        def minus(p, last):
            @pl.when((s <= last) & (zr <= 6 + p))
            def _():
                ring_wait(zr, p)

                @pl.when(s < last)
                def _():
                    ring_copy(ring_piece(zr, p), zr, p, 1, left).start()

                @pl.when(wrapped)
                def _():
                    core_copy(ring_piece(zr, p), zr, p).start()

        def fold_minus():
            @pl.when((s >= 2) & (s - 1 <= 7) & (z + s - 1 >= NZ))
            def _():
                fold_chip(jnp.maximum(z + s - 1 - NZ, 0))

        plus(0, 8)
        minus(0, 7)

        @pl.when(s == 5)
        def _():
            expert(1)

        @pl.when(s == 7)
        def _():
            sum_one_a()

        @pl.when((s >= 2) & (s - 1 <= z))
        def _():
            fold_chip(jnp.maximum(z - s + 1, 0))

        @pl.when(s == 8)
        def _():
            fold_minus()

        plus(1, 7)
        minus(1, 8)

        @pl.when(s == 1)
        def _():
            gather_one()

        @pl.when(s == 2)
        def _():
            gather_two()

        @pl.when(s == 4)
        def _():
            expert(0)

        @pl.when(s == 7)
        def _():
            sum_one_b()

        @pl.when(s < 8)
        def _():
            fold_minus()

        return carry

    lax.fori_loop(1, 10, tick, 0)

    sum_two()

    first = acc[0] / run_sum[0]
    second = acc[1] / run_sum[1]
    diff = first - lam[0, 0] * second
    mean = jnp.mean(diff * diff, axis=0, keepdims=True)
    head_t = diff * lax.rsqrt(mean + norm_eps)
    for load in loads[12:14]:
        load.wait()
    head = (head_t.T * gain[...]).astype(bf16)
    for i in range(NY):
        for j in range(NX):
            at = (i * NX + j) * COLS
            part = jnp.dot(head, wout[:, at:at + COLS], preferred_element_type=f32).astype(bf16)
            at_a[i, j] = part[:ROWS // 2]
            at_b[j, i] = part[ROWS // 2:]
    start_all(at1_a)
    start_all(at1_b)

    three(4, 0, at_a_in).wait_recv()
    for j in range(4):
        t = at_a[y, j].astype(f32)
        for d in range(3):
            t = t + at_a_in[d, j].astype(f32)
        atm_a[j] = t.astype(bf16)
    start_all(at2_a)
    three(4, 1, at_b_in).wait_recv()
    for j in range(4):
        t = at_b[x, j].astype(f32)
        for d in range(3):
            t = t + at_b_in[d, j].astype(f32)
        atm_b[j] = t.astype(bf16)
    start_all(at2_b)

    most = pl.ds(0, NZ - 1)
    remote(
        ret_send.at[most], ret.at[0, most], ret_sent.at[0], ret_came.at[0], partner
    ).wait_recv()
    back = remote(ret.at[0], ret.at[1], pair_send.at[1], pair_recv.at[1], partner)
    back.start()

    back.wait_recv()
    rows = ret[...].reshape(2 * NZ * PAIR, COLS)
    mixture = jnp.dot(pick[0], rows, preferred_element_type=f32) * spread[0]
    mixture = mixture + jnp.dot(pick[1], rows, preferred_element_type=f32) * spread[1]
    expert_out[...] = mixture.astype(bf16)
    results = [
        pltpu.make_async_copy(expert_out, expert_hbm, local_sem.at[14]),
        pltpu.make_async_copy(mixed, mixed_hbm, local_sem.at[15]),
    ]
    results[0].start()

    three(5, 0, atf_a).wait_recv()
    t = atm_a[x].astype(f32)
    for d in range(3):
        t = t + atf_a[d].astype(f32)
    mixed[0:ROWS // 2] = t.astype(bf16)
    three(5, 1, atf_b).wait_recv()
    t = atm_b[y].astype(f32)
    for d in range(3):
        t = t + atf_b[d].astype(f32)
    mixed[ROWS // 2:ROWS] = t.astype(bf16)
    results[1].start()

    exch.wait_send()
    back.wait_send()
    remote(z_send.at[most], z_in.at[most], z_sent.at[0], z_came.at[0], partner).wait_send()
    remote(
        ret_send.at[most], ret.at[0, most], ret_sent.at[0], ret_came.at[0], partner
    ).wait_send()
    for half in range(2):
        three(0, half, ag_a.at[0, pl.ds(0, 3)]).wait_send()
        three(1, half, ag_a.at[pl.ds(0, 3)]).wait_send()
        three(2, half, rs_a_in).wait_send()
        three(3, half, fin_a).wait_send()
        three(4, half, at_a_in).wait_send()
        three(5, half, atf_a).wait_send()

    def sent(way, count):
        if count:
            here = kv.at[pl.ds(0, count)]
            remote(here, here, kv_sent.at[way], core_recv.at[0], partner).wait_send()

    for at in range(NZ):
        @pl.when(z == at)
        def _():
            came_plus = [min(at, 8 - p) for p in range(2)]
            on_plus = [0 if at == NZ - 1 else 1 + min(at, 7 - p) for p in range(2)]
            on_minus = [
                sum((at + s) % NZ <= 6 + p for s in range(7 + p)) for p in range(2)
            ]
            wrapped = [
                sum((at + s) % NZ <= 6 + p and at + s >= NZ for s in range(1, 8 + p))
                for p in range(2)
            ]
            sent(0, sum(on_plus))
            sent(1, sum(on_minus))
            passed = sum(came_plus) + sum(wrapped)

            @pl.when(c == 0)
            def _():
                sent(2, passed + 2)

            @pl.when(c == 1)
            def _():
                sent(2, passed)

    for result in results:
        result.wait()


def call_kernel(*operands):
    hbm = pl.BlockSpec(memory_space=pl.ANY)
    smem = pl.BlockSpec(memory_space=pltpu.SMEM)
    n = HALF * PAIR
    h = ROWS // 2
    V = lambda *shape: pltpu.VMEM(shape, bf16)
    F = lambda *shape: pltpu.VMEM(shape, f32)
    D = lambda *shape: pltpu.SemaphoreType.DMA(shape)
    return pl.pallas_call(
        layer_kernel,
        out_shape=(
            jax.ShapeDtypeStruct((ROWS, COLS), bf16),
            jax.ShapeDtypeStruct((128, COLS), bf16),
        ),
        in_specs=[hbm] * 5 + [smem] + [hbm] * 9,
        out_specs=(hbm, hbm),
        scratch_shapes=[
            V(ROWS, 256), V(ROWS, 256), V(ROWS, 256),
            F(ROWS, 128), F(ROWS, 128), F(1, 256), V(128, 2048), F(1, 2048),
            pltpu.VMEM((2, 128), jnp.int32), F(2, 128),
            V(256, ROWS), V(2, ROWS, ROWS), V(2, NZ, PAIR, COLS), V(2, 128, 2 * NZ * PAIR),
            F(2, 128, 128), V(ROWS, COLS), V(128, COLS),
            V(4 * NZ, ROWS, ROWS),
            pltpu.VMEM((2, ROWS, ROWS), f32),
            pltpu.VMEM((2, 1, ROWS), f32),
            pltpu.VMEM((2, 1, ROWS), f32),
            V(ROWS, 2048), V(2048, 256), V(2048, 256), V(256, 2048),
            V(NZ, PAIR, COLS), V(NZ, PAIR, COLS), V(NZ, PAIR, COLS),
            V(4, 4, HALF, PAIR, COLS), V(4, 4, HALF, PAIR, COLS),
            V(4, 4, n, COLS), V(4, 4, n, COLS), V(3, 4, n, COLS), V(3, 4, n, COLS),
            V(4, n, COLS), V(4, n, COLS), V(3, n, COLS), V(3, n, COLS),
            V(NZ, PAIR, COLS), V(2, NZ, PAIR, COLS),
            V(4, 4, h, COLS), V(4, 4, h, COLS), V(3, 4, h, COLS), V(3, 4, h, COLS),
            V(4, h, COLS), V(4, h, COLS), V(3, h, COLS), V(3, h, COLS),
            D(NZ, 2), D(NZ), D(3), D(2), D(2), D(1), D(1), D(1), D(1), D(6, 2), D(6, 2), D(16),
        ],
        compiler_params=pltpu.CompilerParams(
            collective_id=0, has_side_effects=True, vmem_limit_bytes=60 * 1024 * 1024
        ),
    )(*operands)


def on_device(
    query_maps, key_maps, value_rows, head_lambda, head_gain, out_weight,
    expert_rows, expert_gain, routes, route_weights, gate_weight, up_weight, down_weight,
):
    row_count = query_maps.shape[0]
    positions = lax.axis_index("ep") * row_count + jnp.arange(row_count, dtype=jnp.int32)
    half = jnp.arange(128, dtype=jnp.int32) % 64
    inverse = rope_base ** (-2.0 * half.astype(f32) / 128)
    angles = positions.astype(f32)[:, None] * inverse[None, :]
    sign = jnp.where(jnp.arange(128) < 64, -1.0, 1.0).astype(f32)
    return call_kernel(
        query_maps, key_maps, value_rows, jnp.cos(angles), jnp.sin(angles) * sign,
        head_lambda.reshape(1, 1), head_gain.reshape(1, -1), out_weight, expert_rows,
        expert_gain.reshape(1, -1), routes.T, route_weights.T,
        gate_weight[0], up_weight[0], down_weight[0],
    )


def solution(mesh):
    placed = (
        P("ep", "tp"),
        P("ep", "tp"),
        P("ep", "tp"),
        P("tp"),
        P(),
        P("tp", None),
        P("ep", None),
        P(),
        P("ep", None),
        P("ep", None),
        P("ep", None, "tp"),
        P("ep", None, "tp"),
        P("ep", "tp", None),
    )
    return jax.shard_map(
        on_device,
        mesh=mesh,
        in_specs=placed,
        out_specs=(P("ep", "tp"), P("ep", "tp")),
        check_vma=False,
    )
```

time: 107 us -> 84.1 us (0.79)
  the two profiles are of different devices: /device:TPU:4 before, /device:TPU:481 now
where the time goes in v2:
time: 84.1 us; the launch traced here: 82.8 us
  Pallas kernels  78.1 us (93%)
  local copies, waits for them, and re-layouts  2.1 us (2%)
  between operations  1.31 us (2%)
  other arithmetic  1.25 us (1%)
    pallas_call x1, Pallas kernels, call_kernel(): pl.pallas_call(layer_kernel, out_shape=(jax.ShapeDtypeStruct((ROWS, COLS)...  78.1 us
    unnamed x4, local copies, waits for them, and re-layouts  2.1 us

profile of v2, /device:TPU:481, one launch (start us, length us, event | category | flops | bytes accessed | tf_op | source)
XLA Modules:
  0.0 82.8 jit_solution(17856186071731898033)
XLA Ops:
  1.3 1.2 %fusion = (f32[256,128]{1,0:T(8,128)}, f32[256,128]{1,0:T(8,128)}) fusion(f32[128]{0:T(128)S(1)} %get-tuple-element.4, f32[128]{0:T(128)S(1)} %get-tuple-element.5, f32[256]{0:T(256)S(1)} %add_convert_fusion), kind=kLoop, calls=%fused_computation.2 | loop fusion | flops 65536 | bytes 264192 | tf_op jit(solution)/shard_map/mul | solution.py:592
  2.5 78.1 %shard_map.140 = (bf16[256,128]{1,0:T(8,128)(2,1)}, bf16[128,128]{1,0:T(8,128)(2,1)}) custom-call(bf16[256,256]{1,0:T(8,128)(2,1)} %q_hbm.1, bf16[256,256]{1,0:T(8,128)(2,1)} %k_hbm.1, bf16[256,256]{1,0:T(8,128)(2,1)} %v_hbm.1, f32[256,128]{1,0:T(8,128)} %get-tuple-element.3.cos_hbm, f32[256,128]{1,0:T(8,128)} %get-tuple-element.2.sin_hbm, ...), custom_call_target="tpu_custom_call" | custom-call | tf_op jit(solution)/shard_map/pallas_call | solution.py:547
  80.7 0.0 copy-start
  80.7 1.5 %copy.18 = bf16[256,128]{1,0:T(8,128)(2,1)} copy(bf16[256,128]{1,0:T(8,128)(2,1)} %get-tuple-element.8) | data formatting | bytes 131072
  82.1 0.0 copy-done
  82.1 0.6 copy.19
  (2 shorter events, 0.0 us)
Async XLA Ops:
  80.7 1.5 %copy-start = (bf16[128,128]{1,0:T(8,128)(2,1)S(1)}, bf16[128,128]{1,0:T(8,128)(2,1)}, u32[]{:S(2)}) copy-start(bf16[128,128]{1,0:T(8,128)(2,1)} %get-tuple-element.9) | copy-start | bytes 98308

commit v3 on v2

v3 whole, which is shorter than its diff:
```python
import functools

import jax
import jax.numpy as jnp
import numpy as np
from jax import lax
from jax.experimental import pallas as pl
from jax.experimental.pallas import tpu as pltpu
from jax.sharding import PartitionSpec as P

norm_eps = 1e-06
rope_base = 10000.0
log2e = 1.4426950408889634

NZ = 16
NX = 4
NY = 4
SLOTS = 12
PAIR = 2 * SLOTS
HALF = NZ // 2
ROWS = 256
COLS = 128

MESH = pl.DeviceIdType.MESH
bf16 = jnp.bfloat16
f32 = jnp.float32


def layer_kernel(
    q_hbm, k_hbm, v_hbm, turns_hbm, lam, gain_hbm, wout_hbm, rows_hbm, rgain_hbm,
    routes_hbm, rweights_hbm, gate_hbm, up_hbm, down_hbm,
    mixed, expert_out,
    q_in, k_in, v_in, turns, cos_t, sin_t, gain, row_in, rgain, routes, rweights,
    q_t, kv_own, disp, pick, spread,
    kv, acc, run_max, run_sum, wout, gate_w, up_w, down_w,
    exch_in, z_send, z_in, ag, rs, rs_in, mid, fin,
    ret_send, ret, at_a, at_b, at_a_in, at_b_in, atm_a, atm_b, atf_a, atf_b,
    ring_recv, core_recv, kv_sent, pair_send, pair_recv,
    z_sent, z_came, ret_sent, ret_came, plane_send, plane_recv, tail_send, tail_recv, local_sem, known,
):
    ep = lax.axis_index("ep")
    tp = lax.axis_index("tp")
    z = ep // 2
    c = ep % 2
    y = tp // NX
    x = tp % NX
    partner = (z * 2 + 1 - c, tp)
    right = (((z + 1) % NZ) * 2 + c, tp)
    left = (((z + NZ - 1) % NZ) * 2 + c, tp)

    def z_peer(d):
        return (((z + d) % NZ) * 2 + c, tp)

    def x_peer(d):
        return (ep, y * NX + (x + d) % NX)

    def y_peer(d):
        return (ep, ((y + d) % NY) * NX + x)

    def remote(src, dst, send, recv, device):
        return pltpu.make_async_remote_copy(
            src_ref=src, dst_ref=dst, send_sem=send, recv_sem=recv,
            device_id=device, device_id_type=MESH,
        )

    loads = [
        pltpu.make_async_copy(src, dst, local_sem.at[i])
        for i, (src, dst) in enumerate(
            (
                (turns_hbm, turns), (k_hbm, k_in), (v_hbm, v_in),
                (rows_hbm, row_in), (routes_hbm, routes), (rgain_hbm, rgain), (q_hbm, q_in),
                (rweights_hbm, rweights), (gate_hbm, gate_w), (up_hbm, up_w),
                (down_hbm, down_w), (wout_hbm, wout), (gain_hbm, gain),
            )
        )
    ]

    barrier = pltpu.get_barrier_semaphore()
    for device in (z_peer(2), z_peer(NZ - 2), right, left, partner):
        pl.semaphore_signal(barrier, inc=1, device_id=device, device_id_type=MESH)
    for d in range(1, 4):
        pl.semaphore_signal(barrier, inc=1, device_id=x_peer(d), device_id_type=MESH)
        pl.semaphore_signal(barrier, inc=1, device_id=y_peer(d), device_id_type=MESH)
    for load in loads:
        load.start()

    def tell(i):
        for d in (2 ** (i + 1), NZ - 2 ** (i + 1)):
            pl.semaphore_signal(known.at[i], inc=1, device_id=z_peer(d), device_id_type=MESH)

    def learn(i):
        pl.semaphore_wait(known.at[i], 2)

    def turned(maps, m):
        wide = maps[:, m * 128:(m + 1) * 128].astype(f32)
        return wide * cos_t[...] + pltpu.roll(wide, 64, 1) * sin_t[...]

    loads[0].wait()
    lane = lax.broadcasted_iota(jnp.int32, (128, 128), 1)
    spot = lax.broadcasted_iota(jnp.int32, (128, 128), 0) + jnp.where(lane < 64, 0, 128)
    angles = (ep * ROWS + spot).astype(f32) * turns[...]
    for table, packed in ((cos_t, jnp.cos(angles)), (sin_t, jnp.sin(angles))):
        rolled = pltpu.roll(packed, 64, 1)
        low = -1.0 if table is sin_t else 1.0
        table[0:128] = jnp.where(lane < 64, packed * low, rolled)
        table[128:256] = jnp.where(lane < 64, rolled * low, packed)
    loads[1].wait()
    for m in range(2):
        kv_own[0, :, m * 128:(m + 1) * 128] = turned(k_in, m).astype(bf16)
    loads[2].wait()
    kv_own[1] = v_in[...].astype(f32).T.astype(bf16)
    pl.semaphore_wait(barrier, 5 + 6)
    tell(0)

    def ring_piece(chip, p):
        return kv.at[chip * 4 + c * 2 + p]

    def ring_wait(chip, p):
        here = ring_piece(chip, p)
        remote(here, here, kv_sent.at[0], ring_recv.at[chip, p], left).wait_recv()

    def core_wait(chip):
        here = kv.at[pl.ds(chip * 4 + 2 - c * 2, 2)]
        remote(here, here, kv_sent.at[2], core_recv.at[chip], partner).wait_recv()

    def ring_copy(src, chip, p, way, device):
        return remote(src, ring_piece(chip, p), kv_sent.at[way], ring_recv.at[chip, p], device)

    def core_copy(src, chip, p):
        return remote(src, ring_piece(chip, p), kv_sent.at[2], core_recv.at[chip], partner)

    def send_own(p):
        @pl.when(z < NZ - 1)
        def _():
            ring_copy(kv_own.at[p], z, p, 0, right).start()

        @pl.when(z <= 6 + p)
        def _():
            ring_copy(kv_own.at[p], z, p, 1, left).start()

        @pl.when(c == 0)
        def _():
            core_copy(kv_own.at[p], z, p).start()

    send_own(0)
    send_own(1)

    for i in range(3, 6):
        loads[i].wait()
    wide = row_in[...].astype(f32)
    level = lax.rsqrt(jnp.mean(wide * wide, axis=1, keepdims=True) + norm_eps)
    column = pl.ds(pl.multiple_of(tp * COLS, COLS), COLS)
    normed = (row_in[:, column].astype(f32) * level * rgain[:, column]).astype(bf16)
    chosen = [routes[k:k + 1, :] for k in range(2)]
    names = lax.broadcasted_iota(jnp.int32, (32, 128), 0)
    hot = [(names == r).astype(f32) for r in chosen]
    earlier = (
        lax.broadcasted_iota(jnp.int32, (128, 128), 0)
        < lax.broadcasted_iota(jnp.int32, (128, 128), 1)
    )
    counts = jnp.dot(
        (hot[0] + hot[1]).astype(bf16), earlier.astype(f32).astype(bf16),
        preferred_element_type=f32,
    )
    lines = lax.broadcasted_iota(jnp.int32, (2 * NZ * PAIR, 128), 0).astype(f32)
    base = [
        ((r // 2) * PAIR + c * SLOTS).astype(f32) + jnp.sum(counts * h, axis=0, keepdims=True)
        for r, h in zip(chosen, hot)
    ]
    block = float(NZ * PAIR)
    to_row = [b + (r % 2).astype(f32) * block for b, r in zip(base, chosen)]
    from_row = [
        b + jnp.where(r % 2 == c, 0.0, block) for b, r in zip(base, chosen)
    ]
    spot_of = jnp.where((lines == to_row[0]) | (lines == to_row[1]), 1.0, 0.0).astype(bf16)
    disp[...] = (
        jnp.dot(spot_of, normed, preferred_element_type=f32)
        .astype(bf16)
        .reshape(2, NZ, PAIR, COLS)
    )
    exch = remote(disp.at[1 - c], exch_in, pair_send.at[0], pair_recv.at[0], partner)
    exch.start()
    learn(0)
    tell(1)

    loads[6].wait()
    for m in range(2):
        q_t[m * 128:(m + 1) * 128, :] = turned(q_in, m).T.astype(bf16)
    exch.wait_recv()
    z_send[...] = (disp[c].astype(f32) + exch_in[...].astype(f32)).astype(bf16)
    z_in[z] = z_send[z]
    learn(1)
    for d in range(1, NZ):
        remote(
            z_send.at[(z + d) % NZ], z_in.at[z], z_sent.at[0], z_came.at[0], z_peer(d)
        ).start()
    loads[7].wait()
    for k in range(2):
        pick[k] = jnp.where(lines == from_row[k], 1.0, 0.0).T.astype(bf16)
        spread[k] = jnp.broadcast_to(rweights[k:k + 1, :], (128, 128)).T

    scale = (128 ** -0.5) * log2e

    def fold(k_of, v_of, count, masked, first):
        for m in range(2):
            q_m = q_t[m * 128:(m + 1) * 128, :]
            scores = []
            for i in range(count):
                s = jnp.dot(k_of(i)[:, m * 128:(m + 1) * 128], q_m, preferred_element_type=f32)
                if masked:
                    rows = lax.broadcasted_iota(jnp.int32, s.shape, 0)
                    cols = lax.broadcasted_iota(jnp.int32, s.shape, 1)
                    s = jnp.where(rows <= cols, s, -1e30)
                scores.append(s)
            top = jnp.max(scores[0], axis=0, keepdims=True)
            for s in scores[1:]:
                top = jnp.maximum(top, jnp.max(s, axis=0, keepdims=True))
            top = top * scale
            if first:
                new_max = top
            else:
                old = run_max[m]
                new_max = jnp.maximum(old, top)
                alpha = jnp.exp2(old - new_max)
            total = None
            out = None
            for i in range(count):
                e = jnp.exp2(scores[i] * scale - new_max)
                t = jnp.sum(e, axis=0, keepdims=True)
                total = t if total is None else total + t
                o = jnp.dot(v_of(i), e.astype(bf16), preferred_element_type=f32)
                out = o if out is None else out + o
            run_max[m] = new_max
            if first:
                run_sum[m] = total
                acc[m] = out
            else:
                run_sum[m] = run_sum[m] * alpha + total
                acc[m] = acc[m] * alpha + out

    fold(lambda i: kv_own[0], lambda i: kv_own[1], 1, True, True)

    @pl.when(c == 1)
    def _():
        core_wait(z)
        fold(lambda i: kv[z * 4], lambda i: kv[z * 4 + 1], 1, False, False)

    def fold_chip(chip):
        core_wait(chip)
        fold(
            lambda i: kv[chip * 4 + i * 2], lambda i: kv[chip * 4 + i * 2 + 1], 2, False, False
        )

    place = [(y, x), (x, y)]
    first_peer = (x_peer, y_peer)
    second_peer = (y_peer, x_peer)

    def group_send(phase, g, src_of, dst_of, peer):
        for d in range(1, 4):
            remote(
                src_of(d), dst_of(d), plane_send.at[phase, g], plane_recv.at[phase, g], peer(d)
            ).start()

    def group_three(phase, g, ref):
        return remote(ref, ref, plane_send.at[phase, g], plane_recv.at[phase, g], partner)

    def tail_send_all(phase, half, src_of, dst_of, peer):
        for d in range(1, 4):
            remote(
                src_of(d), dst_of(d), tail_send.at[phase, half], tail_recv.at[phase, half], peer(d)
            ).start()

    def tail_three(phase, half, ref):
        return remote(ref, ref, tail_send.at[phase, half], tail_recv.at[phase, half], partner)

    few = pl.ds(0, 3)

    def gather_one():
        most = pl.ds(0, NZ - 1)
        remote(
            z_send.at[most], z_in.at[most], z_sent.at[0], z_came.at[0], partner
        ).wait_recv()
        for g in range(4):
            u, v = place[g % 2]
            block = pl.ds(4 * g, 4)
            ag[g, u, v] = z_in[block]
            group_send(
                0, g, lambda d: z_in.at[block], lambda d: ag.at[g, u, v], first_peer[g % 2]
            )

    def gather_two():
        for g in range(4):
            u, v = place[g % 2]
            group_three(0, g, ag.at[g, 0, few]).wait_recv()
            group_send(
                1, g, lambda d: ag.at[g, u], lambda d: ag.at[g, u], second_peer[g % 2]
            )

    n = 4 * PAIR

    def expert(r):
        if r == 0:
            for load in loads[8:11]:
                load.wait()
        for g in (2 * r, 2 * r + 1):
            group_three(1, g, ag.at[g, few]).wait_recv()
        pieces = [
            jnp.concatenate(
                [ag[2 * r, i, j].reshape(n, COLS), ag[2 * r + 1, j, i].reshape(n, COLS)], axis=0
            )
            for i in range(NY)
            for j in range(NX)
        ]
        rows = jnp.concatenate(pieces, axis=1)
        gates = jnp.dot(rows, gate_w[...], preferred_element_type=f32)
        ups = jnp.dot(rows, up_w[...], preferred_element_type=f32)
        hidden = (gates / (1.0 + jnp.exp(-gates)) * ups).astype(bf16)
        for i in range(NY):
            for j in range(NX):
                at = (i * NX + j) * COLS
                part = jnp.dot(
                    hidden, down_w[:, at:at + COLS], preferred_element_type=f32
                ).astype(bf16)
                rs[2 * r, i, j] = part[:n]
                rs[2 * r + 1, j, i] = part[n:]
        for g in (2 * r, 2 * r + 1):
            u, v = place[g % 2]
            group_send(
                2, g, lambda d: rs.at[g, (u + d) % 4], lambda d: rs_in.at[g, d - 1],
                second_peer[g % 2],
            )

    def sum_one(r):
        for g in (2 * r, 2 * r + 1):
            u, v = place[g % 2]
            group_three(2, g, rs_in.at[g]).wait_recv()
            for j in range(4):
                t = rs[g, u, j].astype(f32)
                for d in range(3):
                    t = t + rs_in[g, d, j].astype(f32)
                mid[g, j] = t.astype(bf16)
            group_send(
                3, g, lambda d: mid.at[g, (v + d) % 4], lambda d: fin.at[g, d - 1],
                first_peer[g % 2],
            )

    def sum_two(r):
        for g in (2 * r, 2 * r + 1):
            u, v = place[g % 2]
            group_three(3, g, fin.at[g]).wait_recv()
            t = mid[g, v].astype(f32)
            for d in range(3):
                t = t + fin[g, d].astype(f32)
            ret_send[4 * g:4 * g + 4] = t.astype(bf16).reshape(4, PAIR, COLS)
        for to in range(HALF * r, HALF * (r + 1)):
            @pl.when(z == to)
            def _():
                ret[0, to] = ret_send[to]

            @pl.when(z != to)
            def _():
                remote(
                    ret_send.at[to], ret.at[0, z], ret_sent.at[0], ret_came.at[0],
                    (to * 2 + c, tp),
                ).start()

    def tick(s, carry):
        zl = jnp.maximum(z - s, 0)
        zr = (z + s) % NZ
        wrapped = z + s >= NZ

        def plus(p, last):
            @pl.when((s <= last) & (s <= z))
            def _():
                ring_wait(zl, p)

                @pl.when((z < NZ - 1) & (s < last))
                def _():
                    ring_copy(ring_piece(zl, p), zl, p, 0, right).start()

                core_copy(ring_piece(zl, p), zl, p).start()

        def minus(p, last):
            @pl.when((s <= last) & (zr <= 6 + p))
            def _():
                ring_wait(zr, p)

                @pl.when(s < last)
                def _():
                    ring_copy(ring_piece(zr, p), zr, p, 1, left).start()

                @pl.when(wrapped)
                def _():
                    core_copy(ring_piece(zr, p), zr, p).start()

        def fold_minus():
            @pl.when((s >= 2) & (s - 1 <= 7) & (z + s - 1 >= NZ))
            def _():
                fold_chip(jnp.maximum(z + s - 1 - NZ, 0))

        plus(0, 8)
        minus(0, 7)

        @pl.when(s == 5)
        def _():
            expert(0)

        @pl.when(s == 7)
        def _():
            sum_one(0)

        @pl.when(s == 8)
        def _():
            sum_two(0)

        @pl.when(s == 9)
        def _():
            sum_two(1)

        @pl.when((s >= 2) & (s - 1 <= z))
        def _():
            fold_chip(jnp.maximum(z - s + 1, 0))

        @pl.when(s == 8)
        def _():
            fold_minus()

        plus(1, 7)
        minus(1, 8)

        @pl.when(s == 2)
        def _():
            gather_one()

        @pl.when(s == 3)
        def _():
            gather_two()

        @pl.when(s == 5)
        def _():
            expert(1)

        @pl.when(s == 7)
        def _():
            sum_one(1)

        @pl.when(s < 8)
        def _():
            fold_minus()

        return carry

    lax.fori_loop(1, 10, tick, 0)

    first = acc[0] / run_sum[0]
    second = acc[1] / run_sum[1]
    diff = first - lam[0, 0] * second
    mean = jnp.mean(diff * diff, axis=0, keepdims=True)
    head_t = diff * lax.rsqrt(mean + norm_eps)
    for load in loads[11:13]:
        load.wait()
    head = (head_t.T * gain[...]).astype(bf16)
    for i in range(NY):
        for j in range(NX):
            at = (i * NX + j) * COLS
            part = jnp.dot(head, wout[:, at:at + COLS], preferred_element_type=f32).astype(bf16)
            at_a[i, j] = part[:ROWS // 2]
            at_b[j, i] = part[ROWS // 2:]
    tail_send_all(
        0, 0, lambda d: at_a.at[(y + d) % NY], lambda d: at_a_in.at[d - 1], y_peer
    )
    tail_send_all(
        0, 1, lambda d: at_b.at[(x + d) % NX], lambda d: at_b_in.at[d - 1], x_peer
    )

    tail_three(0, 0, at_a_in).wait_recv()
    for j in range(4):
        t = at_a[y, j].astype(f32)
        for d in range(3):
            t = t + at_a_in[d, j].astype(f32)
        atm_a[j] = t.astype(bf16)
    tail_send_all(
        1, 0, lambda d: atm_a.at[(x + d) % NX], lambda d: atf_a.at[d - 1], x_peer
    )
    tail_three(0, 1, at_b_in).wait_recv()
    for j in range(4):
        t = at_b[x, j].astype(f32)
        for d in range(3):
            t = t + at_b_in[d, j].astype(f32)
        atm_b[j] = t.astype(bf16)
    tail_send_all(
        1, 1, lambda d: atm_b.at[(y + d) % NY], lambda d: atf_b.at[d - 1], y_peer
    )

    most = pl.ds(0, NZ - 1)
    remote(
        ret_send.at[most], ret.at[0, most], ret_sent.at[0], ret_came.at[0], partner
    ).wait_recv()
    back = remote(ret.at[0], ret.at[1], pair_send.at[1], pair_recv.at[1], partner)
    back.start()

    back.wait_recv()
    rows = ret[...].reshape(2 * NZ * PAIR, COLS)
    mixture = jnp.dot(pick[0], rows, preferred_element_type=f32) * spread[0]
    mixture = mixture + jnp.dot(pick[1], rows, preferred_element_type=f32) * spread[1]
    expert_out[...] = mixture.astype(bf16)

    tail_three(1, 0, atf_a).wait_recv()
    t = atm_a[x].astype(f32)
    for d in range(3):
        t = t + atf_a[d].astype(f32)
    mixed[0:ROWS // 2] = t.astype(bf16)
    tail_three(1, 1, atf_b).wait_recv()
    t = atm_b[y].astype(f32)
    for d in range(3):
        t = t + atf_b[d].astype(f32)
    mixed[ROWS // 2:ROWS] = t.astype(bf16)

    exch.wait_send()
    back.wait_send()
    remote(z_send.at[most], z_in.at[most], z_sent.at[0], z_came.at[0], partner).wait_send()
    remote(
        ret_send.at[most], ret.at[0, most], ret_sent.at[0], ret_came.at[0], partner
    ).wait_send()
    for g in range(4):
        group_three(0, g, ag.at[g, 0, few]).wait_send()
        group_three(1, g, ag.at[g, few]).wait_send()
        group_three(2, g, rs_in.at[g]).wait_send()
        group_three(3, g, fin.at[g]).wait_send()
    for half in range(2):
        tail_three(0, half, at_a_in).wait_send()
        tail_three(1, half, atf_a).wait_send()

    def sent(way, count):
        if count:
            here = kv.at[pl.ds(0, count)]
            remote(here, here, kv_sent.at[way], core_recv.at[0], partner).wait_send()

    for at in range(NZ):
        @pl.when(z == at)
        def _():
            came_plus = [min(at, 8 - p) for p in range(2)]
            on_plus = [0 if at == NZ - 1 else 1 + min(at, 7 - p) for p in range(2)]
            on_minus = [
                sum((at + s) % NZ <= 6 + p for s in range(7 + p)) for p in range(2)
            ]
            wrapped = [
                sum((at + s) % NZ <= 6 + p and at + s >= NZ for s in range(1, 8 + p))
                for p in range(2)
            ]
            sent(0, sum(on_plus))
            sent(1, sum(on_minus))
            passed = sum(came_plus) + sum(wrapped)

            @pl.when(c == 0)
            def _():
                sent(2, passed + 2)

            @pl.when(c == 1)
            def _():
                sent(2, passed)


def call_kernel(*operands):
    vmem = pl.BlockSpec(memory_space=pltpu.VMEM)
    hbm = pl.BlockSpec(memory_space=pl.ANY)
    smem = pl.BlockSpec(memory_space=pltpu.SMEM)
    n = 4 * PAIR
    h = ROWS // 2
    V = lambda *shape: pltpu.VMEM(shape, bf16)
    F = lambda *shape: pltpu.VMEM(shape, f32)
    D = lambda *shape: pltpu.SemaphoreType.DMA(shape)
    return pl.pallas_call(
        layer_kernel,
        out_shape=(
            pltpu.VMEM((ROWS, COLS), bf16),
            pltpu.VMEM((128, COLS), bf16),
        ),
        in_specs=[hbm] * 4 + [smem] + [hbm] * 9,
        out_specs=(vmem, vmem),
        scratch_shapes=[
            V(ROWS, 256), V(ROWS, 256), V(ROWS, 256),
            F(1, 128), F(ROWS, 128), F(ROWS, 128), F(1, 256), V(128, 2048), F(1, 2048),
            pltpu.VMEM((2, 128), jnp.int32), F(2, 128),
            V(256, ROWS), V(2, ROWS, ROWS), V(2, NZ, PAIR, COLS), V(2, 128, 2 * NZ * PAIR),
            F(2, 128, 128),
            V(4 * NZ, ROWS, ROWS),
            pltpu.VMEM((2, ROWS, ROWS), f32),
            pltpu.VMEM((2, 1, ROWS), f32),
            pltpu.VMEM((2, 1, ROWS), f32),
            V(ROWS, 2048), V(2048, 256), V(2048, 256), V(256, 2048),
            V(NZ, PAIR, COLS), V(NZ, PAIR, COLS), V(NZ, PAIR, COLS),
            V(4, 4, 4, 4, PAIR, COLS), V(4, 4, 4, n, COLS), V(4, 3, 4, n, COLS),
            V(4, 4, n, COLS), V(4, 3, n, COLS),
            V(NZ, PAIR, COLS), V(2, NZ, PAIR, COLS),
            V(4, 4, h, COLS), V(4, 4, h, COLS), V(3, 4, h, COLS), V(3, 4, h, COLS),
            V(4, h, COLS), V(4, h, COLS), V(3, h, COLS), V(3, h, COLS),
            D(NZ, 2), D(NZ), D(3), D(2), D(2), D(1), D(1), D(1), D(1), D(4, 4), D(4, 4), D(2, 2), D(2, 2), D(13),
            pltpu.SemaphoreType.REGULAR((2,)),
        ],
        compiler_params=pltpu.CompilerParams(
            collective_id=0, has_side_effects=True, vmem_limit_bytes=60 * 1024 * 1024
        ),
    )(*operands)


def on_device(
    query_maps, key_maps, value_rows, head_lambda, head_gain, out_weight,
    expert_rows, expert_gain, routes, route_weights, gate_weight, up_weight, down_weight,
):
    turns = rope_base ** (-2.0 * (np.arange(128) % 64) / 128)
    return call_kernel(
        query_maps, key_maps, value_rows, jnp.asarray(turns[None], f32),
        head_lambda.reshape(1, 1), head_gain.reshape(1, -1), out_weight, expert_rows,
        expert_gain.reshape(1, -1), routes.T, route_weights.T,
        gate_weight[0], up_weight[0], down_weight[0],
    )


def solution(mesh):
    placed = (
        P("ep", "tp"),
        P("ep", "tp"),
        P("ep", "tp"),
        P("tp"),
        P(),
        P("tp", None),
        P("ep", None),
        P(),
        P("ep", None),
        P("ep", None),
        P("ep", None, "tp"),
        P("ep", None, "tp"),
        P("ep", "tp", None),
    )
    return jax.shard_map(
        on_device,
        mesh=mesh,
        in_specs=placed,
        out_specs=(P("ep", "tp"), P("ep", "tp")),
        check_vma=False,
    )
```

time: 84.1 us -> 77.6 us (0.923)
  the two profiles are of different devices: /device:TPU:481 before, /device:TPU:449 now
where the time goes in v3:
time: 77.6 us; the launch traced here: 77.4 us
  Pallas kernels  74.9 us (97%)
  between operations  1.29 us (2%)
  local copies, waits for them, and re-layouts  1.25 us (2%)
    pallas_call x1, Pallas kernels, call_kernel(): pl.pallas_call(layer_kernel, out_shape=(pltpu.VMEM((ROWS, COLS), bf16), p...  74.9 us

profile of v3, /device:TPU:449, one launch (start us, length us, event | category | flops | bytes accessed | tf_op | source)
XLA Modules:
  0.0 77.4 jit_solution(11018979702214488649)
XLA Ops:
  1.3 74.9 %shard_map.149 = (bf16[256,128]{1,0:T(8,128)(2,1)S(1)}, bf16[128,128]{1,0:T(8,128)(2,1)S(1)}) custom-call(bf16[256,256]{1,0:T(8,128)(2,1)} %q_hbm.1, bf16[256,256]{1,0:T(8,128)(2,1)} %k_hbm.1, bf16[256,256]{1,0:T(8,128)(2,1)} %v_hbm.1, f32[1,128]{1,0:T(1,128)} %constant.2.clone.turns_hbm, f32[1,1]{1,0:T(1,128)} %bitcast.8.lam, f32[1,256]{1,0:T(1,128)} %bitcast.13, ...), custom_call_target="tpu_custom_call" | custom-call | tf_op jit(solution)/shard_map/pallas_call | solution.py:573
  76.2 0.6 copy.18
  76.8 0.6 copy.19

commit v4 on v3

--- a/solution.py
+++ b/solution.py
@@ -27,14 +27,14 @@
 
 
 def layer_kernel(
-    q_hbm, k_hbm, v_hbm, turns_hbm, lam, gain_hbm, wout_hbm, rows_hbm, rgain_hbm,
+    q_hbm, k_hbm, v_hbm, turns_hbm, lam_hbm, gain_hbm, wout_hbm, rows_hbm, rgain_hbm,
     routes_hbm, rweights_hbm, gate_hbm, up_hbm, down_hbm,
     mixed, expert_out,
-    q_in, k_in, v_in, turns, cos_t, sin_t, gain, row_in, rgain, routes, rweights,
-    q_t, kv_own, disp, pick, spread,
+    q_in, k_in, v_in, turns, cos_t, sin_t, lam, gain, row_in, rgain, routes, rweights,
+    q_t, kv_own, disp, pick, spread, weights,
     kv, acc, run_max, run_sum, wout, gate_w, up_w, down_w,
     exch_in, z_send, z_in, ag, rs, rs_in, mid, fin,
-    ret_send, ret, at_a, at_b, at_a_in, at_b_in, atm_a, atm_b, atf_a, atf_b,
+    ret_send, ret, tail, tail_in, tail_mid, tail_fin,
     ring_recv, core_recv, kv_sent, pair_send, pair_recv,
     z_sent, z_came, ret_sent, ret_came, plane_send, plane_recv, tail_send, tail_recv, local_sem, known,
 ):
@@ -70,7 +70,7 @@
                 (turns_hbm, turns), (k_hbm, k_in), (v_hbm, v_in),
                 (rows_hbm, row_in), (routes_hbm, routes), (rgain_hbm, rgain), (q_hbm, q_in),
                 (rweights_hbm, rweights), (gate_hbm, gate_w), (up_hbm, up_w),
-                (down_hbm, down_w), (wout_hbm, wout), (gain_hbm, gain),
+                (down_hbm, down_w), (wout_hbm, wout), (gain_hbm, gain), (lam_hbm, lam),
             )
         )
     ]
@@ -96,6 +96,8 @@
         return wide * cos_t[...] + pltpu.roll(wide, 64, 1) * sin_t[...]
 
     loads[0].wait()
+    pl.semaphore_wait(barrier, 5 + 6)
+    tell(0)
     lane = lax.broadcasted_iota(jnp.int32, (128, 128), 1)
     spot = lax.broadcasted_iota(jnp.int32, (128, 128), 0) + jnp.where(lane < 64, 0, 128)
     angles = (ep * ROWS + spot).astype(f32) * turns[...]
@@ -109,8 +111,6 @@
         kv_own[0, :, m * 128:(m + 1) * 128] = turned(k_in, m).astype(bf16)
     loads[2].wait()
     kv_own[1] = v_in[...].astype(f32).T.astype(bf16)
-    pl.semaphore_wait(barrier, 5 + 6)
-    tell(0)
 
     def ring_piece(chip, p):
         return kv.at[chip * 4 + c * 2 + p]
@@ -123,11 +123,15 @@
         here = kv.at[pl.ds(chip * 4 + 2 - c * 2, 2)]
         remote(here, here, kv_sent.at[2], core_recv.at[chip], partner).wait_recv()
 
+    def core_wait_one(chip, p, mark):
+        here = kv.at[chip * 4 + 2 - c * 2 + p]
+        remote(here, here, kv_sent.at[2], core_recv.at[mark], partner).wait_recv()
+
     def ring_copy(src, chip, p, way, device):
         return remote(src, ring_piece(chip, p), kv_sent.at[way], ring_recv.at[chip, p], device)
 
-    def core_copy(src, chip, p):
-        return remote(src, ring_piece(chip, p), kv_sent.at[2], core_recv.at[chip], partner)
+    def core_copy(src, chip, p, mark):
+        return remote(src, ring_piece(chip, p), kv_sent.at[2], core_recv.at[mark], partner)
 
     def send_own(p):
         @pl.when(z < NZ - 1)
@@ -140,7 +144,7 @@
 
         @pl.when(c == 0)
         def _():
-            core_copy(kv_own.at[p], z, p).start()
+            core_copy(kv_own.at[p], z, p, z).start()
 
     send_own(0)
     send_own(1)
@@ -189,11 +193,14 @@
     exch.wait_recv()
     z_send[...] = (disp[c].astype(f32) + exch_in[...].astype(f32)).astype(bf16)
     z_in[z] = z_send[z]
-    learn(1)
-    for d in range(1, NZ):
-        remote(
-            z_send.at[(z + d) % NZ], z_in.at[z], z_sent.at[0], z_came.at[0], z_peer(d)
-        ).start()
+
+    def dispatch():
+        learn(1)
+        for d in range(1, NZ):
+            remote(
+                z_send.at[(z + d) % NZ], z_in.at[z], z_sent.at[0], z_came.at[0], z_peer(d)
+            ).start()
+
     loads[7].wait()
     for k in range(2):
         pick[k] = jnp.where(lines == from_row[k], 1.0, 0.0).T.astype(bf16)
@@ -201,7 +208,7 @@
 
     scale = (128 ** -0.5) * log2e
 
-    def fold(k_of, v_of, count, masked, first):
+    def fold(k_of, v_of, count, masked, first, later=False):
         for m in range(2):
             q_m = q_t[m * 128:(m + 1) * 128, :]
             scores = []
@@ -228,15 +235,18 @@
                 e = jnp.exp2(scores[i] * scale - new_max)
                 t = jnp.sum(e, axis=0, keepdims=True)
                 total = t if total is None else total + t
-                o = jnp.dot(v_of(i), e.astype(bf16), preferred_element_type=f32)
-                out = o if out is None else out + o
+                if later:
+                    weights[m, i] = e.astype(bf16)
+                else:
+                    o = jnp.dot(v_of(i), e.astype(bf16), preferred_element_type=f32)
+                    out = o if out is None else out + o
             run_max[m] = new_max
             if first:
                 run_sum[m] = total
                 acc[m] = out
             else:
                 run_sum[m] = run_sum[m] * alpha + total
-                acc[m] = acc[m] * alpha + out
+                acc[m] = acc[m] * alpha if later else acc[m] * alpha + out
 
     fold(lambda i: kv_own[0], lambda i: kv_own[1], 1, True, True)
 
@@ -258,20 +268,20 @@
     def group_send(phase, g, src_of, dst_of, peer):
         for d in range(1, 4):
             remote(
-                src_of(d), dst_of(d), plane_send.at[phase, g], plane_recv.at[phase, g], peer(d)
+                src_of(d), dst_of(d), plane_send.at[phase], plane_recv.at[phase, g], peer(d)
             ).start()
 
     def group_three(phase, g, ref):
-        return remote(ref, ref, plane_send.at[phase, g], plane_recv.at[phase, g], partner)
-
-    def tail_send_all(phase, half, src_of, dst_of, peer):
+        return remote(ref, ref, plane_send.at[phase], plane_recv.at[phase, g], partner)
+
+    def tail_group(phase, g, src_of, dst_of, peer):
         for d in range(1, 4):
             remote(
-                src_of(d), dst_of(d), tail_send.at[phase, half], tail_recv.at[phase, half], peer(d)
+                src_of(d), dst_of(d), tail_send.at[phase], tail_recv.at[phase, g], peer(d)
             ).start()
 
-    def tail_three(phase, half, ref):
-        return remote(ref, ref, tail_send.at[phase, half], tail_recv.at[phase, half], partner)
+    def tail_three(phase, g, ref):
+        return remote(ref, ref, tail_send.at[phase], tail_recv.at[phase, g], partner)
 
     few = pl.ds(0, 3)
 
@@ -344,15 +354,14 @@
                 first_peer[g % 2],
             )
 
-    def sum_two(r):
-        for g in (2 * r, 2 * r + 1):
-            u, v = place[g % 2]
-            group_three(3, g, fin.at[g]).wait_recv()
-            t = mid[g, v].astype(f32)
-            for d in range(3):
-                t = t + fin[g, d].astype(f32)
-            ret_send[4 * g:4 * g + 4] = t.astype(bf16).reshape(4, PAIR, COLS)
-        for to in range(HALF * r, HALF * (r + 1)):
+    def sum_two(g):
+        u, v = place[g % 2]
+        group_three(3, g, fin.at[g]).wait_recv()
+        t = mid[g, v].astype(f32)
+        for d in range(3):
+            t = t + fin[g, d].astype(f32)
+        ret_send[4 * g:4 * g + 4] = t.astype(bf16).reshape(4, PAIR, COLS)
+        for to in range(4 * g, 4 * g + 4):
             @pl.when(z == to)
             def _():
                 ret[0, to] = ret_send[to]
@@ -378,7 +387,7 @@
                 def _():
                     ring_copy(ring_piece(zl, p), zl, p, 0, right).start()
 
-                core_copy(ring_piece(zl, p), zl, p).start()
+                core_copy(ring_piece(zl, p), zl, p, zl).start()
 
         def minus(p, last):
             @pl.when((s <= last) & (zr <= 6 + p))
@@ -391,39 +400,50 @@
 
                 @pl.when(wrapped)
                 def _():
-                    core_copy(ring_piece(zr, p), zr, p).start()
+                    mark = jnp.where(s == 8, NZ, zr)
+                    core_copy(ring_piece(zr, p), zr, p, mark).start()
 
         def fold_minus():
             @pl.when((s >= 2) & (s - 1 <= 7) & (z + s - 1 >= NZ))
             def _():
                 fold_chip(jnp.maximum(z + s - 1 - NZ, 0))
 
+        @pl.when(s == 5)
+        def _():
+            expert(0)
+
         plus(0, 8)
         minus(0, 7)
 
-        @pl.when(s == 5)
-        def _():
-            expert(0)
+        @pl.when(s == 1)
+        def _():
+            dispatch()
 
         @pl.when(s == 7)
         def _():
+            sum_one(1)
+
+        @pl.when((s == 7) & (z >= 8))
+        def _():
+            sum_two(0)
+
+        @pl.when((s >= 2) & (s - 1 <= z))
+        def _():
+            fold_chip(jnp.maximum(z - s + 1, 0))
+
+        @pl.when(s == 8)
+        def _():
+            fold_minus()
+
+        @pl.when(s == 6)
+        def _():
             sum_one(0)
 
-        @pl.when(s == 8)
-        def _():
-            sum_two(0)
-
-        @pl.when(s == 9)
-        def _():
-            sum_two(1)
-
-        @pl.when((s >= 2) & (s - 1 <= z))
-        def _():
-            fold_chip(jnp.maximum(z - s + 1, 0))
-
-        @pl.when(s == 8)
-        def _():
-            fold_minus()
+        @pl.when((s == 8) & (z >= 8))
+        def _():
+            far = jnp.maximum(z - 8, 0)
+            core_wait_one(far, 0, far)
+            fold(lambda i: kv[far * 4 + i * 2], None, 2, False, False, later=True)
 
         plus(1, 7)
         minus(1, 8)
@@ -440,57 +460,74 @@
         def _():
             expert(1)
 
-        @pl.when(s == 7)
-        def _():
-            sum_one(1)
-
         @pl.when(s < 8)
         def _():
             fold_minus()
 
         return carry
 
-    lax.fori_loop(1, 10, tick, 0)
-
+    lax.fori_loop(1, 9, tick, 0)
+
+    @pl.when(z >= 8)
+    def _():
+        sum_two(1)
+        sum_two(2)
+        sum_two(3)
+        far = jnp.maximum(z - 8, 0)
+        core_wait_one(far, 1, NZ)
+        for m in range(2):
+            out = jnp.dot(kv[far * 4 + 1], weights[m, 0], preferred_element_type=f32)
+            acc[m] = acc[m] + (
+                out + jnp.dot(kv[far * 4 + 3], weights[m, 1], preferred_element_type=f32)
+            )
+
+
+    @pl.when(z < 8)
+    def _():
+        sum_two(0)
+        sum_two(1)
+
+    for load in loads[11:14]:
+        load.wait()
     first = acc[0] / run_sum[0]
     second = acc[1] / run_sum[1]
-    diff = first - lam[0, 0] * second
+    diff = first - lam[...] * second
     mean = jnp.mean(diff * diff, axis=0, keepdims=True)
     head_t = diff * lax.rsqrt(mean + norm_eps)
-    for load in loads[11:13]:
-        load.wait()
-    head = (head_t.T * gain[...]).astype(bf16)
-    for i in range(NY):
-        for j in range(NX):
-            at = (i * NX + j) * COLS
-            part = jnp.dot(head, wout[:, at:at + COLS], preferred_element_type=f32).astype(bf16)
-            at_a[i, j] = part[:ROWS // 2]
-            at_b[j, i] = part[ROWS // 2:]
-    tail_send_all(
-        0, 0, lambda d: at_a.at[(y + d) % NY], lambda d: at_a_in.at[d - 1], y_peer
-    )
-    tail_send_all(
-        0, 1, lambda d: at_b.at[(x + d) % NX], lambda d: at_b_in.at[d - 1], x_peer
-    )
-
-    tail_three(0, 0, at_a_in).wait_recv()
-    for j in range(4):
-        t = at_a[y, j].astype(f32)
-        for d in range(3):
-            t = t + at_a_in[d, j].astype(f32)
-        atm_a[j] = t.astype(bf16)
-    tail_send_all(
-        1, 0, lambda d: atm_a.at[(x + d) % NX], lambda d: atf_a.at[d - 1], x_peer
-    )
-    tail_three(0, 1, at_b_in).wait_recv()
-    for j in range(4):
-        t = at_b[x, j].astype(f32)
-        for d in range(3):
-            t = t + at_b_in[d, j].astype(f32)
-        atm_b[j] = t.astype(bf16)
-    tail_send_all(
-        1, 1, lambda d: atm_b.at[(y + d) % NY], lambda d: atf_b.at[d - 1], y_peer
-    )
+    for half in range(2):
+        head = (head_t[:, half * 128:(half + 1) * 128].T * gain[...]).astype(bf16)
+        for i in range(NY):
+            for j in range(NX):
+                at = (i * NX + j) * COLS
+                part = jnp.dot(
+                    head, wout[:, at:at + COLS], preferred_element_type=f32
+                ).astype(bf16)
+                tail[2 * half, i, j] = part[:64]
+                tail[2 * half + 1, j, i] = part[64:]
+        for g in (2 * half, 2 * half + 1):
+            u, v = place[g % 2]
+            tail_group(
+                0, g, lambda d: tail.at[g, (u + d) % 4], lambda d: tail_in.at[g, d - 1],
+                second_peer[g % 2],
+            )
+
+    for g in range(4):
+        u, v = place[g % 2]
+        tail_three(0, g, tail_in.at[g]).wait_recv()
+        for j in range(4):
+            t = tail[g, u, j].astype(f32)
+            for d in range(3):
+                t = t + tail_in[g, d, j].astype(f32)
+            tail_mid[g, j] = t.astype(bf16)
+        tail_group(
+            1, g, lambda d: tail_mid.at[g, (v + d) % 4], lambda d: tail_fin.at[g, d - 1],
+            first_peer[g % 2],
+        )
+        if g == 1:
+            @pl.when(z < 8)
+            def _():
+                sum_two(2)
+                sum_two(3)
 
     most = pl.ds(0, NZ - 1)
     remote(
@@ -505,16 +542,12 @@
     mixture = mixture + jnp.dot(pick[1], rows, preferred_element_type=f32) * spread[1]
     expert_out[...] = mixture.astype(bf16)
 
-    tail_three(1, 0, atf_a).wait_recv()
-    t = atm_a[x].astype(f32)
-    for d in range(3):
-        t = t + atf_a[d].astype(f32)
-    mixed[0:ROWS // 2] = t.astype(bf16)
-    tail_three(1, 1, atf_b).wait_recv()
-    t = atm_b[y].astype(f32)
-    for d in range(3):
-        t = t + atf_b[d].astype(f32)
-    mixed[ROWS // 2:ROWS] = t.astype(bf16)
+    for g in range(4):
+        tail_three(1, g, tail_fin.at[g]).wait_recv()
+        t = tail_mid[g, place[g % 2][1]].astype(f32)
+        for d in range(3):
+            t = t + tail_fin[g, d].astype(f32)
+        mixed[64 * g:64 * (g + 1)] = t.astype(bf16)
 
     exch.wait_send()
     back.wait_send()
@@ -522,14 +555,12 @@
     remote(
         ret_send.at[most], ret.at[0, most], ret_sent.at[0], ret_came.at[0], partner
     ).wait_send()
-    for g in range(4):
-        group_three(0, g, ag.at[g, 0, few]).wait_send()
-        group_three(1, g, ag.at[g, few]).wait_send()
-        group_three(2, g, rs_in.at[g]).wait_send()
-        group_three(3, g, fin.at[g]).wait_send()
-    for half in range(2):
-        tail_three(0, half, at_a_in).wait_send()
-        tail_three(1, half, atf_a).wait_send()
+    group_three(0, 0, ag.at[0, few]).wait_send()
+    group_three(1, 0, ag.at[few]).wait_send()
+    group_three(2, 0, rs_in).wait_send()
+    group_three(3, 0, fin).wait_send()
+    tail_three(0, 0, tail_in).wait_send()
+    tail_three(1, 0, tail_fin).wait_send()
 
     def sent(way, count):
         if count:
@@ -564,9 +595,8 @@
 def call_kernel(*operands):
     vmem = pl.BlockSpec(memory_space=pltpu.VMEM)
     hbm = pl.BlockSpec(memory_space=pl.ANY)
-    smem = pl.BlockSpec(memory_space=pltpu.SMEM)
     n = 4 * PAIR
-    h = ROWS // 2
+    h = ROWS // 4
     V = lambda *shape: pltpu.VMEM(shape, bf16)
     F = lambda *shape: pltpu.VMEM(shape, f32)
     D = lambda *shape: pltpu.SemaphoreType.DMA(shape)
@@ -576,14 +606,14 @@
             pltpu.VMEM((ROWS, COLS), bf16),
             pltpu.VMEM((128, COLS), bf16),
         ),
-        in_specs=[hbm] * 4 + [smem] + [hbm] * 9,
+        in_specs=[hbm] * 14,
         out_specs=(vmem, vmem),
         scratch_shapes=[
             V(ROWS, 256), V(ROWS, 256), V(ROWS, 256),
-            F(1, 128), F(ROWS, 128), F(ROWS, 128), F(1, 256), V(128, 2048), F(1, 2048),
+            F(1, 128), F(ROWS, 128), F(ROWS, 128), F(1, 1), F(1, 256), V(128, 2048), F(1, 2048),
             pltpu.VMEM((2, 128), jnp.int32), F(2, 128),
             V(256, ROWS), V(2, ROWS, ROWS), V(2, NZ, PAIR, COLS), V(2, 128, 2 * NZ * PAIR),
-            F(2, 128, 128),
+            F(2, 128, 128), V(2, 2, ROWS, ROWS),
             V(4 * NZ, ROWS, ROWS),
             pltpu.VMEM((2, ROWS, ROWS), f32),
             pltpu.VMEM((2, 1, ROWS), f32),
@@ -593,9 +623,8 @@
             V(4, 4, 4, 4, PAIR, COLS), V(4, 4, 4, n, COLS), V(4, 3, 4, n, COLS),
             V(4, 4, n, COLS), V(4, 3, n, COLS),
             V(NZ, PAIR, COLS), V(2, NZ, PAIR, COLS),
-            V(4, 4, h, COLS), V(4, 4, h, COLS), V(3, 4, h, COLS), V(3, 4, h, COLS),
-            V(4, h, COLS), V(4, h, COLS), V(3, h, COLS), V(3, h, COLS),
-            D(NZ, 2), D(NZ), D(3), D(2), D(2), D(1), D(1), D(1), D(1), D(4, 4), D(4, 4), D(2, 2), D(2, 2), D(13),
+            V(4, 4, 4, h, COLS), V(4, 3, 4, h, COLS), V(4, 4, h, COLS), V(4, 3, h, COLS),
+            D(NZ, 2), D(NZ + 1), D(3), D(2), D(2), D(1), D(1), D(1), D(1), D(4), D(4, 4), D(2), D(2, 4), D(14),
             pltpu.SemaphoreType.REGULAR((2,)),
         ],
         compiler_params=pltpu.CompilerParams(

time: 77.6 us -> 75.8 us (0.977)
  the two profiles are of different devices: /device:TPU:449 before, /device:TPU:256 now
where the time goes in v4:
time: 75.8 us; the launch traced here: 75.7 us
  Pallas kernels  73.2 us (97%)
  between operations  1.29 us (2%)
  local copies, waits for them, and re-layouts  1.25 us (2%)
    pallas_call x1, Pallas kernels, call_kernel(): pl.pallas_call(layer_kernel, out_shape=(pltpu.VMEM((ROWS, COLS), bf16), p...  73.2 us

profile of v4, /device:TPU:256, one launch (start us, length us, event | category | flops | bytes accessed | tf_op | source)
XLA Modules:
  0.0 75.7 jit_solution(1307376962543261354)
XLA Ops:
  1.3 73.2 %shard_map.149 = (bf16[256,128]{1,0:T(8,128)(2,1)S(1)}, bf16[128,128]{1,0:T(8,128)(2,1)S(1)}) custom-call(bf16[256,256]{1,0:T(8,128)(2,1)} %q_hbm.1, bf16[256,256]{1,0:T(8,128)(2,1)} %k_hbm.1, bf16[256,256]{1,0:T(8,128)(2,1)} %v_hbm.1, f32[1,128]{1,0:T(1,128)} %constant.2.clone.turns_hbm, f32[1,1]{1,0:T(1,128)} %bitcast.8.lam_hbm, f32[1,256]{1,0:T(1,128)} %bitcast.13, ...), custom_call_target="tpu_custom_call" | custom-call | tf_op jit(solution)/shard_map/pallas_call | solution.py:603
  74.5 0.6 copy.18
  75.1 0.6 copy.19

commit v5 on v4

--- a/solution.py
+++ b/solution.py
@@ -138,9 +138,9 @@
         def _():
             ring_copy(kv_own.at[p], z, p, 0, right).start()
 
-        @pl.when(z <= 6 + p)
-        def _():
-            ring_copy(kv_own.at[p], z, p, 1, left).start()
+        @pl.when(z <= 7 - p)
+        def _():
+            ring_copy(kv_own.at[1 - p], z, 1 - p, 1, left).start()
 
         @pl.when(c == 0)
         def _():
@@ -412,8 +412,18 @@
         def _():
             expert(0)
 
+        def fold_plus():
+            @pl.when((s >= 2) & (s - 1 <= z))
+            def _():
+                fold_chip(jnp.maximum(z - s + 1, 0))
+
+        @pl.when((s == 8) & (c == 0))
+        def _():
+            fold_plus()
+            fold_minus()
+
         plus(0, 8)
-        minus(0, 7)
+        minus(1, 8)
 
         @pl.when(s == 1)
         def _():
@@ -427,11 +437,11 @@
         def _():
             sum_two(0)
 
-        @pl.when((s >= 2) & (s - 1 <= z))
-        def _():
-            fold_chip(jnp.maximum(z - s + 1, 0))
-
-        @pl.when(s == 8)
+        @pl.when((s < 8) | (c == 1))
+        def _():
+            fold_plus()
+
+        @pl.when((s == 8) & (c == 1))
         def _():
             fold_minus()
 
@@ -446,7 +456,7 @@
             fold(lambda i: kv[far * 4 + i * 2], None, 2, False, False, later=True)
 
         plus(1, 7)
-        minus(1, 8)
+        minus(0, 7)
 
         @pl.when(s == 2)
         def _():

time: 75.8 us -> 74.6 us (0.984)
  the two profiles are of different devices: /device:TPU:256 before, /device:TPU:481 now
where the time goes in v5:
time: 74.6 us; the launch traced here: 74.5 us
  Pallas kernels  72 us (97%)
  between operations  1.29 us (2%)
  local copies, waits for them, and re-layouts  1.25 us (2%)
    pallas_call x1, Pallas kernels, call_kernel(): pl.pallas_call(layer_kernel, out_shape=(pltpu.VMEM((ROWS, COLS), bf16), p...  72 us

profile of v5, /device:TPU:481, one launch (start us, length us, event | category | flops | bytes accessed | tf_op | source)
XLA Modules:
  0.0 74.5 jit_solution(14957470984008275233)
XLA Ops:
  1.3 72.0 %shard_map.149 = (bf16[256,128]{1,0:T(8,128)(2,1)S(1)}, bf16[128,128]{1,0:T(8,128)(2,1)S(1)}) custom-call(bf16[256,256]{1,0:T(8,128)(2,1)} %q_hbm.1, bf16[256,256]{1,0:T(8,128)(2,1)} %k_hbm.1, bf16[256,256]{1,0:T(8,128)(2,1)} %v_hbm.1, f32[1,128]{1,0:T(1,128)} %constant.2.clone.turns_hbm, f32[1,1]{1,0:T(1,128)} %bitcast.8.lam_hbm, f32[1,256]{1,0:T(1,128)} %bitcast.13, ...), custom_call_target="tpu_custom_call" | custom-call | tf_op jit(solution)/shard_map/pallas_call | solution.py:613
  73.3 0.6 copy.18
  73.9 0.6 copy.19

commit v6 on v5

--- a/solution.py
+++ b/solution.py
@@ -75,13 +75,15 @@
         )
     ]
 
+    for load in loads[:3]:
+        load.start()
     barrier = pltpu.get_barrier_semaphore()
     for device in (z_peer(2), z_peer(NZ - 2), right, left, partner):
         pl.semaphore_signal(barrier, inc=1, device_id=device, device_id_type=MESH)
     for d in range(1, 4):
         pl.semaphore_signal(barrier, inc=1, device_id=x_peer(d), device_id_type=MESH)
         pl.semaphore_signal(barrier, inc=1, device_id=y_peer(d), device_id_type=MESH)
-    for load in loads:
+    for load in loads[3:]:
         load.start()
 
     def tell(i):
@@ -481,8 +483,6 @@
     @pl.when(z >= 8)
     def _():
         sum_two(1)
-        sum_two(2)
-        sum_two(3)
         far = jnp.maximum(z - 8, 0)
         core_wait_one(far, 1, NZ)
         for m in range(2):
@@ -499,9 +499,7 @@
 
     for load in loads[11:14]:
         load.wait()
-    first = acc[0] / run_sum[0]
-    second = acc[1] / run_sum[1]
-    diff = first - lam[...] * second
+    diff = acc[0] * (1.0 / run_sum[0]) - acc[1] * (lam[...] / run_sum[1])
     mean = jnp.mean(diff * diff, axis=0, keepdims=True)
     head_t = diff * lax.rsqrt(mean + norm_eps)
     for half in range(2):
@@ -520,6 +518,11 @@
                 0, g, lambda d: tail.at[g, (u + d) % 4], lambda d: tail_in.at[g, d - 1],
                 second_peer[g % 2],
             )
+
+    @pl.when(z >= 8)
+    def _():
+        sum_two(2)
+        sum_two(3)
 
     for g in range(4):
         u, v = place[g % 2]

time: 74.6 us -> 74.5 us (level)
  no operation moved by 1% of the time
where the time goes in v6:
time: 74.5 us; the launch traced here: 74.3 us
  Pallas kernels  71.8 us (96%)
  between operations  1.29 us (2%)
  local copies, waits for them, and re-layouts  1.25 us (2%)
    pallas_call x1, Pallas kernels, call_kernel(): pl.pallas_call(layer_kernel, out_shape=(pltpu.VMEM((ROWS, COLS), bf16), p...  71.8 us

profile of v6, /device:TPU:481, one launch (start us, length us, event | category | flops | bytes accessed | tf_op | source)
XLA Modules:
  0.0 74.3 jit_solution(10313305605078460126)
XLA Ops:
  1.3 71.8 %shard_map.149 = (bf16[256,128]{1,0:T(8,128)(2,1)S(1)}, bf16[128,128]{1,0:T(8,128)(2,1)S(1)}) custom-call(bf16[256,256]{1,0:T(8,128)(2,1)} %q_hbm.1, bf16[256,256]{1,0:T(8,128)(2,1)} %k_hbm.1, bf16[256,256]{1,0:T(8,128)(2,1)} %v_hbm.1, f32[1,128]{1,0:T(1,128)} %constant.2.clone.turns_hbm, f32[1,1]{1,0:T(1,128)} %bitcast.8.lam_hbm, f32[1,256]{1,0:T(1,128)} %bitcast.13, ...), custom_call_target="tpu_custom_call" | custom-call | tf_op jit(solution)/shard_map/pallas_call | solution.py:616
  73.1 0.6 copy.18
  73.7 0.6 copy.19
